TPU v7x, 128 devices: a whole 4x4x4 slice. The times are simulated.
128 devices in a mesh: sp: 16 (over z, y), tp: 8 (over x, core).
Axes of the slice: x: 4, y: 4, z: 4, core: 2. Of those that a mesh axis runs over, the one named last changes fastest.
Arguments:
- resid: bfloat16 [16384, 2048], P(('sp', 'tp')), may hold values from -6 to 6
- query_nope: bfloat16 [16384, 2048], P('sp', 'tp'), may hold values from -18 to 18
- query_rope: bfloat16 [16384, 1024], P('sp', 'tp'), may hold values from -300 to 300
- latent: bfloat16 [16384, 256], P('sp'), may hold values from -6 to 6
- key_rope: bfloat16 [16384, 64], P('sp'), may hold values from -6 to 6
- latent_gain: float32 [256], replicated, may hold values from 0.1 to 1.9
- w_key: bfloat16 [256, 2048], P(None, 'tp'), may hold values from -0.375 to 0.375
- w_value: bfloat16 [256, 2048], P(None, 'tp'), may hold values from -0.375 to 0.375
- w_out: bfloat16 [2048, 2048], P('tp'), may hold values from -0.125 to 0.125
- mix_gain: float32 [2048], replicated, may hold values from 0.1 to 1.9
- w_gate: bfloat16 [2048, 5632], P('sp', 'tp'), may hold values from -0.125 to 0.125
- w_up: bfloat16 [2048, 5632], P('sp', 'tp'), may hold values from -0.125 to 0.125
- w_down: bfloat16 [2048, 5632], P('sp', 'tp'), may hold values from -0.078125 to 0.078125
Outputs:
- layer_out: bfloat16 [16384, 2048], P(('sp', 'tp'))
All inputs are finite; a program needn't handle non-finite values.
Results may differ from a plain program's by a relative error of at most 0.0095.
Values may be sent and summed in bfloat16 or wider, within the bound.
A program may use at most 128 MiB of HBM per device.

v0:
```python
import jax
import jax.numpy as jnp
from jax import lax
from jax.sharding import PartitionSpec as P

NOPE = 128
ROPE = 64
VDIM = 128


norm_eps = 1e-06
masked_score = -1e30
theta_base = 10000.0


def in_one_piece(arrays, axis, dim, along):
    both = jnp.concatenate(arrays, axis=along)
    filled, at, gathered = (lax.all_gather(both, axis, axis=dim, tiled=True), 0, [])
    for a in arrays:
        gathered.append(lax.slice_in_dim(filled, at, at + a.shape[along], axis=along))
        at += a.shape[along]
    return tuple(gathered)


def split_up(array, dim, count):
    lengths = array.shape
    tiles = array.reshape(*lengths[:dim], count, lengths[dim] // count, *lengths[dim + 1 :])
    return jnp.moveaxis(tiles, dim, 0)


def summed_on_arrival(array, axis, dim):
    tiles = split_up(array, dim, lax.axis_size(axis))
    arrived = lax.all_to_all(tiles, axis, split_axis=0, concat_axis=0, tiled=True)
    return arrived.astype(jnp.float32).sum(axis=0)


def rotate(values_in, angle):
    half_width = values_in.shape[-1] // 2
    front_half = values_in[..., :half_width]
    back_half = values_in[..., half_width:]
    cosine = jnp.cos(angle)
    sine_part = jnp.sin(angle)
    return jnp.concatenate(
        [front_half * cosine - back_half * sine_part, back_half * cosine + front_half * sine_part],
        axis=-1,
    )


def angles(positions, full_width):
    half_width = full_width // 2
    frequency = theta_base ** (-2.0 * jnp.arange(half_width).astype(jnp.float32) / full_width)
    return positions[:, None] * frequency[None, :]


def rms_scale(values_in, gain):
    return (
        values_in
        * lax.rsqrt(jnp.mean(values_in * values_in, axis=-1, keepdims=True) + norm_eps)
        * gain
    )


def attend(fold_state, queries, key_block, value_block, rope_block, block_start):
    nope_query, rope_query, query_rows = queries
    running_max, weight_sum, accumulated = fold_state
    key_rows = block_start + jnp.arange(key_block.shape[0], dtype=jnp.int32)
    causal = key_rows[None, :] <= query_rows[:, None]
    scores = jnp.einsum("qhd,khd->hqk", nope_query, key_block, preferred_element_type=jnp.float32)
    scores = scores + jnp.einsum(
        "qhr,kr->hqk", rope_query, rope_block, preferred_element_type=jnp.float32
    )
    scores = jnp.where(causal[None], scores * (NOPE + ROPE) ** (-0.5), masked_score)
    new_max = jnp.maximum(running_max, jnp.max(scores, axis=-1))
    weights = jnp.where(causal[None], jnp.exp(scores - new_max[..., None]), 0.0)
    factor = jnp.exp(running_max - new_max)
    weight_sum = weight_sum * factor + jnp.sum(weights, axis=-1)
    accumulated = accumulated * factor[..., None] + jnp.einsum(
        "hqk,khd->hqd",
        weights.astype(jnp.bfloat16),
        value_block,
        preferred_element_type=jnp.float32,
    )
    return (new_max, weight_sum, accumulated)


def over_blocks(fold_state, arrays, last_query, step_fn, row_count):
    piece_rows = arrays[0].shape[0]
    candidates = [
        row_count * multiple
        for multiple in (4, 2, 1)
        if piece_rows % (row_count * multiple) == 0 and row_count * multiple <= 2048
    ]
    block_rows = candidates[0]
    block_count = piece_rows // block_rows
    stacked = tuple(
        (member.reshape((block_count, block_rows) + member.shape[1:]) for member in arrays)
    )

    def advance(state_in, indexed):
        block_index, blocks_now = indexed
        block_start = block_index * block_rows

        def compute(state_now):
            return step_fn(state_now, blocks_now, block_start)

        def unchanged(state_now):
            return state_now

        return (lax.cond(block_start <= last_query, compute, unchanged, state_in), None)

    result, ignored = lax.scan(
        advance, fold_state, (jnp.arange(block_count, dtype=jnp.int32), stacked)
    )
    return result


def on_device(
    resid,
    query_nope,
    query_rope,
    latent,
    key_rope,
    latent_gain,
    w_key,
    w_value,
    w_out,
    mix_gain,
    w_gate,
    w_up,
    w_down,
):
    row_count = query_nope.shape[0]
    head_count = query_nope.shape[1] // NOPE
    first_row = lax.axis_index("sp") * row_count
    query_rows = first_row + jnp.arange(row_count, dtype=jnp.int32)
    angle = angles(query_rows.astype(jnp.float32), ROPE)
    nope_query = query_nope.reshape(row_count, head_count, NOPE)
    rope_query = rotate(
        query_rope.astype(jnp.float32).reshape(row_count, head_count, ROPE), angle[:, None, :]
    ).astype(jnp.bfloat16)
    latent_normed = rms_scale(latent.astype(jnp.float32), latent_gain).astype(jnp.bfloat16)
    key_rotated = rotate(key_rope.astype(jnp.float32), angle).astype(jnp.bfloat16)
    queries = (nope_query, rope_query, query_rows)
    last_query = first_row + row_count - 1
    initial = (
        jnp.full((head_count, row_count), masked_score, jnp.float32),
        jnp.zeros((head_count, row_count), jnp.float32),
        jnp.zeros((head_count, row_count, VDIM), jnp.float32),
    )
    gate_full, up_full, down_full = in_one_piece((w_gate, w_up, w_down), "sp", 0, 1)

    def expand_block(state_now, blocks_now, block_start):
        latent_block, rope_block = blocks_now
        key_block = jnp.dot(latent_block, w_key, preferred_element_type=jnp.float32).astype(
            jnp.bfloat16
        )
        value_block = jnp.dot(latent_block, w_value, preferred_element_type=jnp.float32).astype(
            jnp.bfloat16
        )
        return attend(
            state_now,
            queries,
            key_block.reshape(-1, head_count, NOPE),
            value_block.reshape(-1, head_count, VDIM),
            rope_block,
            block_start,
        )

    final_state = over_blocks(
        initial,
        in_one_piece((latent_normed, key_rotated), "sp", 0, 1),
        last_query,
        expand_block,
        row_count,
    )
    head_out = (final_state[2] / final_state[1][..., None]).astype(jnp.bfloat16)
    out_heads = w_out.reshape(head_count, VDIM, w_out.shape[1])
    part_rows = head_out
    head_term = jnp.einsum("hqv,hvd->qd", part_rows, out_heads, preferred_element_type=jnp.float32)
    attention_proj = summed_on_arrival(
        lax.optimization_barrier(head_term.astype(jnp.bfloat16))
        .astype(jnp.float32)
        .astype(jnp.bfloat16),
        "tp",
        0,
    )
    stream = resid.astype(jnp.float32) + attention_proj
    normed = rms_scale(stream, mix_gain).astype(jnp.bfloat16)
    row_piece = lax.all_gather(normed, "tp", axis=0, tiled=True)
    gate_value = jnp.dot(row_piece, gate_full, preferred_element_type=jnp.float32)
    upward = jnp.dot(row_piece, up_full, preferred_element_type=jnp.float32)
    hidden = (jax.nn.silu(gate_value) * upward).astype(jnp.bfloat16)
    part_rows = hidden
    down_term = lax.dot_general(
        part_rows, down_full, (((1,), (1,)), ((), ())), preferred_element_type=jnp.float32
    )
    mixer_out = lax.psum_scatter(
        lax.optimization_barrier(down_term.astype(jnp.bfloat16))
        .astype(jnp.float32)
        .astype(jnp.bfloat16),
        "tp",
        scatter_dimension=0,
        tiled=True,
    ).astype(jnp.float32)
    return (stream + 0.5 * mixer_out).astype(jnp.bfloat16)


def solution(mesh):
    return jax.shard_map(
        on_device,
        mesh=mesh,
        in_specs=(
            P(("sp", "tp"), None),
            P("sp", "tp"),
            P("sp", "tp"),
            P("sp", None),
            P("sp", None),
            P(),
            P(None, "tp"),
            P(None, "tp"),
            P("tp", None),
            P(),
            P("sp", "tp"),
            P("sp", "tp"),
            P("sp", "tp"),
        ),
        out_specs=P(("sp", "tp"), None),
        check_vma=False,
    )
```

profile of v0, /device:TPU:1, one launch (start us, length us, event | category | flops | bytes accessed | tf_op | source)
XLA Modules:
  0.0 637.7 jit_solution(16293472215441492424)
XLA Ops:
  8.6 1.3 fusion.31
  9.9 1.2 fusion.33
  11.2 1.1 pad_maximum_fusion
  14.7 90.7 %all-gather.4.cloned.1.call-done = bf16[16384,320]{1,0:T(8,128)(2,1)} async-done(((bf16[1024,320]{1,0:T(8,128)(2,1)}), bf16[16384,320]{1,0:T(8,128)(2,1)}) %all-gather.4.cloned.1.call-update) | async-done | bytes 10485776 | tf_op jit(solution)/shard_map/all_gather | solution.py:18
  105.4 3.7 slice.39
  109.1 4.8 copy.29
  113.8 7.1 %slice.38 = bf16[16384,256]{1,0:T(8,128)(2,1)} slice(bf16[16384,320]{1,0:T(8,128)(2,1)} %all-gather.4.cloned.1.call-done), slice={[0:16384], [0:256]} | slice | bytes 16777216 | tf_op jit(solution)/shard_map/slice | solution.py:20
  123.2 59.4 %while.15 = (s32[]{:T(128)}, f32[2,1024]{1,0:T(2,128)S(1)}, f32[2,1024]{1,0:T(2,128)}, f32[2,1024,128]{2,1,0:T(8,128)}, s32[8]{0:T(128)}, /*index=5*/s32[]{:T(12...) while((s32[]{:T(128)}, f32[2,1024]{1,0:T(2,128)S(1)}, ...), condition=%wide.region_6.7_spmd.clone, body=%wide.region_1.6_spmd.clone.sunk | while | flops 3266845696 | bytes 178161584 | solution.py:111
  123.2 1.3 dynamic_slice.38
  125.1 43.7 %conditional.3 = ((f32[2,1024]{1,0:T(2,128)S(1)}, f32[2,1024]{1,0:T(2,128)}, f32[2,1024,128]{2,1,0:T(8,128)})) conditional(s32[]{:T(128)} %convert_element_type.126, (f32[2,1024]{1,0:T(2,128)S(1)}, f32[2,1024]{1,0:T(2,128)}, f32[2,1024,128]{2,1,0:T(8,128)}) %tuple.44, (s32[]{:T(128)}, s32[]{:T(128)}, bf16[8,2048,256]{2,1,0:T(8,128)(2,1)}, s32[]{:T(128)}, ...), branch_computations={%region_2.2_spmd, %region_3.5_spmd} | conditional | flops 3266845696 | bytes 178157184 | solution.py:109
  125.2 1.8 convolution_convert_fusion.1
  126.9 8.1 %fusion.37 = f32[2,2048,1024]{2,1,0:T(8,128)} fusion(bf16[2048,2,128]{0,2,1:T(8,128)(2,1)S(1)} %bitcast.42, bf16[1024,2,128]{2,0,1:T(8,128)(2,1)S(1)} %get-tuple-element.152), kind=kOutput, calls=%fused_computation.62 | convolution fusion | flops 1073741824 | bytes 18350080 | tf_op jit(solution)/shard_map/while/body/eval_jaxpr/cond/branch_1_fun/qhd,khd->hqk/dot_general | solution.py:68
  135.1 1.3 broadcast_compare_fusion
  136.4 12.3 %fusion.36 = (f32[2,1024]{1,0:T(2,128)S(1)}, f32[2,1024,2048]{1,2,0:T(8,128)}) fusion(bf16[1024,2,64]{0,2,1:T(8,128)(2,1)} %get-tuple-element.154, bf16[8,2048,64]{1,2,0:T(8,128)(2,1)} %get-tuple-element.153, s32[]{:T(128)} %get-tuple-element.150, f32[2,2048,1024]{2,1,0:T(8,128)} %fusion.37, pred[1024,2048]{0,1:T(8,128)(4,1)S(1)} %broadcast_compare_fusion), kind=kOutput, calls=%fused_computation.61 | convolution fusion | flops 553646080 | bytes 36184576 | tf_op jit(solution)/shard_map/while/body/eval_jaxpr/cond/branch_1_fun/qhr,kr->hqk/dot_general | solution.py:69
  148.8 8.6 %fusion.5 = f32[2,1024]{1,0:T(2,128)S(1)} fusion(f32[2,1024,2048]{1,2,0:T(8,128)} %get-tuple-element.256, f32[2,1024]{1,0:T(2,128)S(1)} %max.4, pred[1024,2048]{0,1:T(8,128)(4,1)} %copy-done.2), kind=kLoop, calls=%fused_computation.6 | loop fusion | flops 12580864 | bytes 18890752 | tf_op jit(solution)/shard_map/while/body/eval_jaxpr/cond/branch_1_fun/reduce_sum | solution.py:76
  157.4 2.1 multiply_add_fusion
  159.4 1.8 convolution_convert_fusion
  161.2 7.7 %fusion.9 = f32[2,1024,128]{2,1,0:T(8,128)} fusion(bf16[2048,2,128]{0,2,1:T(8,128)(2,1)S(1)} %bitcast.44, f32[2,1024,2048]{1,2,0:T(8,128)S(1)} %copy-done.1, f32[2,1024]{1,0:T(2,128)S(1)} %max.4, pred[1024,2048]{0,1:T(8,128)(4,1)} %copy-done.2, f32[2,1024,128]{2,1,0:T(8,128)} %get-tuple-element.156, f32[2,1024]{1,0:T(2,128)S(1)} %get-tuple-element.254), kind=kOutput, calls=%fused_computation.12 | convolution fusion | flops 1086849024 | bytes 22036480 | tf_op jit(solution)/shard_map/while/body/eval_jaxpr/cond/branch_1_fun/hqk,khd->hqd/dot_general | solution.py:77
  168.9 1.3 dynamic_slice.38
  170.8 1.3 dynamic_slice.38
  172.8 1.3 dynamic_slice.38
  174.8 1.3 dynamic_slice.38
  176.7 1.3 dynamic_slice.38
  178.7 1.3 dynamic_slice.38
  180.7 1.3 dynamic_slice.38
  182.6 2.5 bitcast_convert_fusion
  185.2 53.5 %all_to_all.5 = bf16[8,128,2048]{2,1,0:T(8,128)(2,1)S(1)} all-to-all(bf16[8,128,2048]{2,1,0:T(8,128)(2,1)S(1)} %bitcast.46), channel_id=1, replica_groups=mesh['sp'=16,'tp'=8] {'tp'}, dimensions={0} | all-to-all | bytes 8388608 | tf_op jit(solution)/shard_map/all_to_all | solution.py:33
  241.0 333.4 %all-gather.6.cloned.1.call-done = bf16[1024,2048]{1,0:T(8,128)(2,1)} async-done(((bf16[128,2048]{1,0:T(8,128)(2,1)}), bf16[1024,2048]{1,0:T(8,128)(2,1)}) %all-gather.6.cloned.1.call-update) | async-done | bytes 4194320 | tf_op jit(solution)/shard_map/all_gather | solution.py:189
  574.5 7.9 %fusion.25 = f32[1024,704]{0,1:T(8,128)} fusion(bf16[1024,2048]{1,0:T(8,128)(2,1)} %all-gather.6.cloned.1.call-done, bf16[2048,2112]{0,1:T(8,128)(2,1)} %all-gather.8.cloned.1.call-done), kind=kOutput, calls=%fused_computation.33 | convolution fusion | flops 2952790016 | bytes 9961472 | tf_op jit(solution)/shard_map/dot_general | solution.py:190
  582.4 12.0 %convolution_convert_fusion.2 = bf16[1024,2048]{1,0:T(8,128)(2,1)} fusion(bf16[2048,2112]{0,1:T(8,128)(2,1)} %all-gather.8.cloned.1.call-done, f32[1024,704]{0,1:T(8,128)} %fusion.25, bf16[1024,2048]{1,0:T(8,128)(2,1)} %all-gather.6.cloned.1.call-done), kind=kOutput, calls=%fused_computation.29 | convolution fusion | flops 5912002560 | bytes 17039360 | tf_op jit(solution)/shard_map/dot_general | solution.py:194
  594.4 34.7 %reduce-scatter.2.cloned.1.call-done = bf16[128,2048]{1,0:T(8,128)(2,1)} async-done(((bf16[1024,2048]{1,0:T(8,128)(2,1)}), bf16[128,2048]{1,0:T(8,128)(2,1)}) %reduce-scatter.2.cloned.1.call-update) | async-done | bytes 524304 | tf_op jit(solution)/shard_map/reduce_scatter | solution.py:197
  629.1 2.0 add_convert_fusion
  (71 shorter events, 9.1 us)
Async XLA Ops:
  6.5 176.1 %copy-start = (bf16[256,2048]{1,0:T(8,128)(2,1)S(1)}, bf16[256,2048]{1,0:T(8,128)(2,1)}, u32[]{:S(2)}) copy-start(bf16[256,2048]{1,0:T(8,128)(2,1)} %param.25) | copy-start | bytes 3145732
  6.5 5.8 copy-start.9
  6.5 5.8 copy-start.8
  6.5 5.8 copy-start.7
  6.5 6.7 %copy-start.6 = (bf16[1024,128]{1,0:T(8,128)(2,1)S(1)}, bf16[1024,128]{1,0:T(8,128)(2,1)}, u32[]{:S(2)}) copy-start(bf16[1024,128]{1,0:T(8,128)(2,1)} %param.19) | copy-start | bytes 786436
  6.5 6.9 %copy-start.5 = (bf16[1024,256]{1,0:T(8,128)(2,1)S(1)}, bf16[1024,256]{1,0:T(8,128)(2,1)}, u32[]{:S(2)}) copy-start(bf16[1024,256]{1,0:T(8,128)(2,1)} %param.18) | copy-start | bytes 1572868
  6.6 98.8 %all-gather.4.cloned.1.call-start = ((), (), s32[]{:S(2)}) async-start(), calls=%async_computation.2 | async-start | bytes 13369344 | tf_op jit(solution)/shard_map/all_gather | solution.py:18
  12.3 228.7 %all-gather.8.cloned.1.call-start = ((), (), s32[]{:S(2)}) async-start(), calls=%async_computation.4 | async-start | bytes 9191424 | tf_op jit(solution)/shard_map/all_gather | solution.py:18
  13.2 561.2 %all-gather.6.cloned.1.call-start = ((), (), s32[]{:S(2)}) async-start(), calls=%async_computation.3 | async-start | bytes 4718592 | tf_op jit(solution)/shard_map/all_gather | solution.py:189
  136.4 12.3 %copy-start.2 = (pred[1024,2048]{0,1:T(8,128)(4,1)}, pred[1024,2048]{0,1:T(8,128)(4,1)S(1)}, u32[]{:S(2)}) copy-start(pred[1024,2048]{0,1:T(8,128)(4,1)S(1)} %broadcast_compare_fusion) | copy-start | bytes 6291460 | tf_op jit(solution)/shard_map/while/body/eval_jaxpr/cond
  148.7 10.7 %copy-start.4 = (bf16[256,256]{1,0:T(8,128)(2,1)S(1)}, bf16[256,256]{1,0:T(8,128)(2,1)}, u32[]{:S(2)}) copy-start(bf16[256,256]{1,0:T(8,128)(2,1)} %get-tuple-element.157) | copy-start | bytes 393220 | tf_op jit(solution)/shard_map/while/body/eval_jaxpr/cond
  148.7 12.5 %copy-start.1 = (f32[2,1024,2048]{1,2,0:T(8,128)S(1)}, f32[2,1024,2048]{1,2,0:T(8,128)}, u32[]{:S(2)}) copy-start(f32[2,1024,2048]{1,2,0:T(8,128)} %get-tuple-element.256) | copy-start | bytes 50331652 | tf_op jit(solution)/shard_map/while/body/eval_jaxpr/cond
  238.7 1.0 copy-start.3
  238.7 1.3 copy-start.10
  241.0 388.2 %reduce-scatter.2.cloned.1.call-start = ((), (), s32[]{:S(2)}) async-start(), calls=%async_computation.5 | async-start | bytes 4718592 | tf_op jit(solution)/shard_map/reduce_scatter | solution.py:197
Sparse Core Ops, SparseCore 0:
  12.4 92.9 all-gather.3
  107.5 77.0 all-gather.7
  241.1 333.3 all-gather.5
  594.5 34.5 reduce-scatter.1
where the time goes:
time: 641 us; the launch traced here: 638 us
  waiting for transfers between devices  459 us (72%)
  matrix products  54.1 us (8%)
  blocking collectives  53.5 us (8%)
  local copies, waits for them, and re-layouts  29.3 us (5%)
  other arithmetic  22.9 us (4%)
  between operations  13.3 us (2%)
    all_gather x1, waiting for transfers between devices, on_device(): row_piece = lax.all_gather(normed, 'tp', axis=0, tiled=True)  333 us
    all_gather x2, waiting for transfers between devices, in_one_piece(): lax.all_gather(both, axis, axis=dim, tiled=True)  90.7 us
    all_to_all x1, blocking collectives, summed_on_arrival(): lax.all_to_all(tiles, axis, split_axis=0, concat_axis=0, tiled=True)  53.5 us
    reduce_scatter x1, waiting for transfers between devices, on_device(): lax.psum_scatter(lax.optimization_barrier(down_term.astype(jnp.bfloat16))...  34.7 us
  transfers between devices with their start and end apart: 4, of which 3 were waited for; matrix products, arithmetic and copies ran while one was open for 12% of the time, Pallas kernels for 0%

commit v1 on v0

v1 whole, which is shorter than its diff:
```python
import functools

import jax
import jax.numpy as jnp
from jax import lax
from jax.experimental import pallas as pl
from jax.experimental.pallas import tpu as pltpu
from jax.sharding import PartitionSpec as P

NOPE = 128
ROPE = 64
VDIM = 128
ROWS = 1024
HALF = 512
SIDE = 4
SHARD = HALF + HALF // 4

norm_eps = 1e-06
masked_score = -1e30
theta_base = 10000.0
score_base2 = (NOPE + ROPE) ** (-0.5) * 1.4426950408889634
MESH = pl.DeviceIdType.MESH

ORDER = ((0, 0), (1, 0), (3, 0), (0, 1), (0, 3), (2, 0), (0, 2), (1, 1), (1, 3), (3, 1), (3, 3),
         (2, 1), (2, 3), (1, 2), (3, 2), (2, 2))
PLACE = {pair: p for p, pair in enumerate(ORDER)}
ALPHA, BETA, FULL = (0, 320), (320, 320), (0, 640)
ALPHA0, ALPHA1, BETA0, BETA1 = (0, 160), (160, 160), (320, 160), (480, 160)

SENDS = (
    (((0, 0), FULL, (1, 0), 0), ((0, 0), FULL, (-1, 0), 0), ((0, 0), FULL, (0, 1), 0), ((0, 0), FULL, (0, -1), 0)),
    (
        ((1, 0), ALPHA, (-1, 0), 0), ((3, 0), BETA, (1, 0), 1),
        ((0, 1), ALPHA, (0, -1), 0), ((0, 3), BETA, (0, 1), 1),
        ((1, 0), ALPHA, (0, 1), 0), ((1, 0), ALPHA, (0, -1), 0),
        ((3, 0), ALPHA, (0, 1), 0), ((3, 0), ALPHA, (0, -1), 0),
        ((0, 1), BETA, (1, 0), 1), ((0, 1), BETA, (-1, 0), 1),
        ((0, 3), BETA, (1, 0), 1), ((0, 3), BETA, (-1, 0), 1),
    ),
    (
        ((2, 0), ALPHA, (0, 1), 0), ((2, 0), ALPHA, (0, -1), 0),
        ((0, 2), BETA, (1, 0), 1), ((0, 2), BETA, (-1, 0), 1),
    ),
    (
        ((1, 1), ALPHA0, (0, -1), 0), ((1, 3), ALPHA1, (0, 1), 2),
        ((3, 1), ALPHA0, (0, -1), 0), ((3, 3), ALPHA1, (0, 1), 2),
        ((1, 1), BETA0, (-1, 0), 1), ((3, 1), BETA1, (1, 0), 2),
        ((1, 3), BETA0, (-1, 0), 1), ((3, 3), BETA1, (1, 0), 2),
    ),
    (
        ((2, 1), ALPHA0, (0, -1), 0), ((2, 3), ALPHA1, (0, 1), 1),
        ((1, 2), BETA0, (-1, 0), 2), ((3, 2), BETA1, (1, 0), 3),
    ),
)


def at_receiver(source, step):
    return PLACE[((source[0] - step[0]) % SIDE, (source[1] - step[1]) % SIDE)]


def pick(index, values):
    found = jnp.int32(values[0])
    for at in range(1, len(values)):
        found = jnp.where(index == at, jnp.int32(values[at]), found)
    return found


def attention_kernel(
    nope, rope, shard, w_key, w_value, w_out, heads_all, w_out_all,
    lat, far_nope, far_rope, queries, keys, values_t, w_value_t, top, total, acc, head_out,
    send_sem, recv_sem, pair_send, pair_recv, query_send, query_recv, head_send, head_recv,
    out_send, out_recv, local_sem,
):
    s = lax.axis_index("sp")
    t = lax.axis_index("tp")
    z, y = s // SIDE, s % SIDE
    x, core = t // 2, t % 2
    mirror = 15 - s

    def sp_at(dy, dz):
        return ((z + dz + SIDE) % SIDE) * SIDE + (y + dy + SIDE) % SIDE

    def tp_at(dx):
        return ((x + dx + SIDE) % SIDE) * 2 + core

    partner = x * 2 + 1 - core

    barrier = pltpu.get_barrier_semaphore()
    for step in (1, 2, 3):
        pl.semaphore_signal(barrier, inc=1, device_id=(sp_at(step, 0), t), device_id_type=MESH)
        pl.semaphore_signal(barrier, inc=1, device_id=(sp_at(0, step), t), device_id_type=MESH)
    for step in range(1, 8):
        pl.semaphore_signal(barrier, inc=1, device_id=(s, (t + step) % 8), device_id_type=MESH)
    for step in range(8):
        pl.semaphore_signal(barrier, inc=1, device_id=(mirror, (t + step) % 8), device_id_type=MESH)
    pl.semaphore_wait(barrier, 21)

    def query_copies():
        return (
            pltpu.make_async_remote_copy(
                nope.at[pl.ds(HALF, HALF)], far_nope, query_send.at[0], query_recv.at[0],
                device_id=(mirror, t), device_id_type=MESH),
            pltpu.make_async_remote_copy(
                rope.at[pl.ds(HALF, HALF)], far_rope, query_send.at[1], query_recv.at[1],
                device_id=(mirror, t), device_id_type=MESH),
        )

    for copy in query_copies():
        copy.start()

    own = 2 * s + core

    def relative(pair, plane):
        return 2 * sp_at(*pair) + plane

    def shard_copy(phase, index):
        source, (first, count), step, slot = SENDS[phase][index]
        number = sum(len(one) for one in SENDS[:phase]) + index
        place = at_receiver(source, step)
        block = relative(source, core)
        if phase == 0:
            source_ref = shard
        else:
            source_ref = lat.at[block, pl.ds(first, count)]
        return pltpu.make_async_remote_copy(
            source_ref, lat.at[block, pl.ds(first, count)],
            send_sem.at[number], recv_sem.at[4 * place + slot],
            device_id=(sp_at(*step), t), device_id_type=MESH)

    def start_phase(phase):
        for index in range(len(SENDS[phase])):
            shard_copy(phase, index).start()

    def wait_received(phase):
        for index, (source, (first, count), step, slot) in enumerate(SENDS[phase]):
            place = at_receiver(source, step)
            block = relative(ORDER[place], core)
            pltpu.make_async_remote_copy(
                lat.at[block, pl.ds(first, count)], lat.at[block, pl.ds(first, count)],
                send_sem.at[0], recv_sem.at[4 * place + slot],
                device_id=(sp_at(*step), t), device_id_type=MESH).wait_recv()

    def pair_copy(place):
        block = relative(ORDER[place], core)
        return pltpu.make_async_remote_copy(
            shard if place == 0 else lat.at[block], lat.at[block],
            pair_send.at[place], pair_recv.at[place],
            device_id=(s, partner), device_id_type=MESH)

    def out_copy(number, slot, rows, target):
        first, count = rows
        source = w_out.at[pl.ds(first, count)] if number < 3 else w_out_all.at[slot, pl.ds(first, count)]
        return pltpu.make_async_remote_copy(
            source, w_out_all.at[slot, pl.ds(first, count)],
            out_send.at[number], out_recv.at[number],
            device_id=(s, target), device_id_type=MESH)

    whole, upper, lower = (0, 256), (0, 128), (128, 128)
    right, left, across = tp_at(1), tp_at(3), tp_at(2)
    out_sends = (
        (0, t, whole, right), (1, t, whole, left), (2, t, whole, partner),
        (3, right, upper, left), (4, left, lower, right),
        (5, right, whole, partner), (6, left, whole, partner), (7, across, whole, partner),
    )

    def other(slot):
        return (slot // 2) * 2 + 1 - slot % 2

    out_receives = (
        (0, left, whole), (1, right, whole), (2, partner, whole),
        (3, across, upper), (4, across, lower),
        (5, other(right), whole), (6, other(left), whole), (7, other(across), whole),
    )

    def out_wait(number):
        _, slot, (first, count) = out_receives[number]
        pltpu.make_async_remote_copy(
            w_out_all.at[slot, pl.ds(first, count)], w_out_all.at[slot, pl.ds(first, count)],
            out_send.at[number], out_recv.at[number],
            device_id=(s, partner), device_id_type=MESH).wait_recv()

    start_phase(0)
    pair_copy(0).start()
    for number in range(3):
        out_copy(*out_sends[number]).start()
    own_shard = pltpu.make_async_copy(shard, lat.at[own], local_sem.at[0])
    own_shard.start()
    own_out = pltpu.make_async_copy(w_out, w_out_all.at[t], local_sem.at[1])
    own_out.start()

    w_value_t[...] = jnp.transpose(w_value[...].astype(jnp.float32)).astype(jnp.bfloat16)
    top[...] = jnp.full_like(top, masked_score)
    total[...] = jnp.zeros_like(total)
    acc[...] = jnp.zeros_like(acc)

    lanes = lax.broadcasted_iota(jnp.int32, (HALF, 128), 1)

    def set_queries(group, nope_rows, rope_rows):
        wide = rope_rows.astype(jnp.float32)
        turned = pltpu.roll(wide, 64, 1)
        front = lanes < 64
        for head in range(2):
            one = nope_rows[:, head * NOPE:(head + 1) * NOPE]
            low, high = (wide, turned) if head == 0 else (turned, wide)
            for version, tail in enumerate((jnp.where(front, low, 0.0), jnp.where(front, 0.0, high))):
                queries[group, head, version, :, 0:NOPE] = one
                queries[group, head, version, :, NOPE:2 * NOPE] = tail.astype(jnp.bfloat16)

    set_queries(0, nope[pl.ds(0, HALF), :], rope[pl.ds(0, HALF), :])
    own_shard.wait()
    for copy in query_copies():
        copy.wait_recv()
    set_queries(1, far_nope[...], far_rope[...])

    last_near, last_far = 2 * s, 31 - 2 * s

    def expand(block):
        rows = lat[block, pl.ds(0, HALF), :]
        expanded = jnp.dot(rows, w_key[...], preferred_element_type=jnp.float32).astype(jnp.bfloat16)
        tails = (lat[block, pl.ds(HALF, 128), 0:128], lat[block, pl.ds(HALF, 128), 128:256])
        for head in range(2):
            keys[head, :, 0:NOPE] = expanded[:, head * NOPE:(head + 1) * NOPE]
            for quarter in range(4):
                keys[head, pl.ds(quarter * 128, 128), NOPE:2 * NOPE] = tails[quarter % 2]
        values_t[...] = lax.dot_general(
            w_value_t[...], rows, (((1,), (1,)), ((), ())), preferred_element_type=jnp.float32
        ).astype(jnp.bfloat16)

    def fold(group, masked):
        for head in range(2):
            scores = jnp.concatenate(
                [
                    lax.dot_general(
                        keys[head, pl.ds(256 * version, 256), :], queries[group, head, version],
                        (((1,), (1,)), ((), ())), preferred_element_type=jnp.float32)
                    for version in range(2)
                ],
                axis=0,
            )
            if masked:
                key_at = lax.broadcasted_iota(jnp.int32, scores.shape, 0)
                query_at = lax.broadcasted_iota(jnp.int32, scores.shape, 1)
                scores = jnp.where(key_at <= query_at, scores, masked_score)
            before = top[group, head]
            after = jnp.maximum(before, jnp.max(scores, axis=0, keepdims=True))
            weights = jnp.exp2(scores * score_base2 - after * score_base2)
            factor = jnp.exp2((before - after) * score_base2)
            total[group, head] = total[group, head] * factor + jnp.sum(weights, axis=0, keepdims=True)
            acc[group, head] = acc[group, head] * factor + jnp.dot(
                values_t[head * VDIM:(head + 1) * VDIM, :], weights.astype(jnp.bfloat16),
                preferred_element_type=jnp.float32)
            top[group, head] = after

    def process(block):
        @pl.when(block <= jnp.maximum(last_near, last_far))
        def _():
            expand(block)

        def one(group, carry):
            last = jnp.where(group == 0, last_near, last_far)

            @pl.when(block < last)
            def _():
                fold(group, False)

            @pl.when(block == last)
            def _():
                fold(group, True)

            return carry

        lax.fori_loop(0, 2, one, 0)

    def advance(place, carry):
        @pl.when(place == 1)
        def _():
            wait_received(0)
            start_phase(1)
            for at in (1, 2, 3, 4):
                pair_copy(at).start()

        @pl.when(place == 3)
        def _():
            wait_some(1, 0, 4)
            start_phase(2)
            for at in (5, 6):
                pair_copy(at).start()

        @pl.when(place == 5)
        def _():
            wait_some(1, 4, 12)
            start_phase(3)
            for at in (7, 8, 9, 10):
                pair_copy(at).start()

        @pl.when(place == 7)
        def _():
            out_wait(0)
            out_wait(1)
            for number in (3, 4, 5, 6):
                out_copy(*out_sends[number]).start()

        @pl.when(place == 8)
        def _():
            wait_received(2)
            wait_received(3)
            start_phase(4)
            for at in (11, 12, 13, 14):
                pair_copy(at).start()

        @pl.when(place == 13)
        def _():
            wait_received(4)
            pair_copy(15).start()
            out_wait(3)
            out_wait(4)
            out_copy(*out_sends[7]).start()

        dy = pick(place, [pair[0] for pair in ORDER])
        dz = pick(place, [pair[1] for pair in ORDER])
        base = 2 * sp_at(dy, dz)

        def plane(turn, carry):
            block = base + (core + turn) % 2

            @pl.when(turn == 1)
            def _():
                pltpu.make_async_remote_copy(
                    lat.at[block], lat.at[block], pair_send.at[place], pair_recv.at[place],
                    device_id=(s, partner), device_id_type=MESH).wait_recv()

            process(block)
            return carry

        lax.fori_loop(0, 2, plane, 0)
        return carry

    def wait_some(phase, first_index, last_index):
        for source, (first, count), step, slot in SENDS[phase][first_index:last_index]:
            place = at_receiver(source, step)
            block = relative(ORDER[place], core)
            pltpu.make_async_remote_copy(
                lat.at[block, pl.ds(first, count)], lat.at[block, pl.ds(first, count)],
                send_sem.at[0], recv_sem.at[4 * place + slot],
                device_id=(sp_at(*step), t), device_id_type=MESH).wait_recv()

    lax.fori_loop(0, 16, advance, 0)

    for group in range(2):
        for head in range(2):
            mixed = acc[group, head] / total[group, head]
            head_out[group, :, head * VDIM:(head + 1) * VDIM] = jnp.transpose(mixed).astype(jnp.bfloat16)

    def head_copy(group, part):
        target = part if group == 0 else 4 + part
        return pltpu.make_async_remote_copy(
            head_out.at[group, pl.ds(128 * part, 128)], heads_all.at[t],
            head_send.at[4 * group + part], head_recv.at[t],
            device_id=(s if group == 0 else mirror, target), device_id_type=MESH)

    for part in range(4):
        head_copy(1, part).start()

        @pl.when(t != part)
        def _():
            head_copy(0, part).start()

    @pl.when(t < 4)
    def _():
        mine = pltpu.make_async_copy(
            head_out.at[0, pl.ds(128 * (t % 4), 128)], heads_all.at[t], local_sem.at[2])
        mine.start()
        mine.wait()

    def head_wait(slot, carry):
        @pl.when((t >= 4) | (slot != t))
        def _():
            pltpu.make_async_remote_copy(
                head_out.at[0, pl.ds(0, 128)], heads_all.at[slot], head_send.at[0], head_recv.at[slot],
                device_id=(mirror, t), device_id_type=MESH).wait_recv()

        return carry

    lax.fori_loop(0, 8, head_wait, 0)

    own_out.wait()
    for number in (2, 5, 6, 7):
        out_wait(number)
    for number in range(8):
        out_copy(*out_sends[number]).wait_send()
    for copy in query_copies():
        copy.wait_send()
    for phase in range(len(SENDS)):
        for index in range(len(SENDS[phase])):
            shard_copy(phase, index).wait_send()
    for place in range(16):
        pair_copy(place).wait_send()
    for part in range(4):
        head_copy(1, part).wait_send()

        @pl.when(t != part)
        def _():
            head_copy(0, part).wait_send()


def attention_call(nope, rope, shard, w_key, w_value, w_out):
    vmem = pl.BlockSpec(memory_space=pltpu.VMEM)
    anywhere = pl.BlockSpec(memory_space=pl.ANY)
    dma = pltpu.SemaphoreType.DMA
    bf16, f32 = jnp.bfloat16, jnp.float32
    return pl.pallas_call(
        attention_kernel,
        out_shape=(
            jax.ShapeDtypeStruct((8, 128, 256), bf16),
            jax.ShapeDtypeStruct((8, 256, 2048), bf16),
        ),
        in_specs=[vmem] * 5 + [anywhere],
        out_specs=[anywhere, anywhere],
        scratch_shapes=[
            pltpu.VMEM((32, SHARD, 256), bf16),
            pltpu.VMEM((HALF, 256), bf16),
            pltpu.VMEM((HALF, 128), bf16),
            pltpu.VMEM((2, 2, 2, HALF, 256), bf16),
            pltpu.VMEM((2, HALF, 256), bf16),
            pltpu.VMEM((256, HALF), bf16),
            pltpu.VMEM((256, 256), bf16),
            pltpu.VMEM((2, 2, 1, HALF), f32),
            pltpu.VMEM((2, 2, 1, HALF), f32),
            pltpu.VMEM((2, 2, VDIM, HALF), f32),
            pltpu.VMEM((2, HALF, 256), bf16),
            dma((32,)), dma((64,)), dma((16,)), dma((16,)), dma((2,)), dma((2,)), dma((8,)), dma((8,)),
            dma((8,)), dma((8,)), dma((3,)),
        ],
        compiler_params=pltpu.CompilerParams(
            collective_id=0, has_side_effects=True, vmem_limit_bytes=48 * 1024 * 1024),
        cost_estimate=pl.CostEstimate(flops=60_000_000_000, bytes_accessed=30_000_000, transcendentals=18_000_000),
        name="attention",
    )(nope, rope, shard, w_key, w_value, w_out)


def rotate(values_in, cosine, sine_part):
    half_width = values_in.shape[-1] // 2
    front_half = values_in[..., :half_width]
    back_half = values_in[..., half_width:]
    return jnp.concatenate(
        [front_half * cosine - back_half * sine_part, back_half * cosine + front_half * sine_part],
        axis=-1,
    )


def angles(positions, full_width):
    half_width = full_width // 2
    frequency = theta_base ** (-2.0 * jnp.arange(half_width).astype(jnp.float32) / full_width)
    return positions[:, None] * frequency[None, :]


def rms_scale(values_in, gain):
    return (
        values_in
        * lax.rsqrt(jnp.mean(values_in * values_in, axis=-1, keepdims=True) + norm_eps)
        * gain
    )


def on_device(
    resid, query_nope, query_rope, latent, key_rope, latent_gain, w_key, w_value, w_out, mix_gain,
    w_gate, w_up, w_down,
):
    gate_full = lax.all_gather(w_gate, "sp", axis=0, tiled=True)
    up_full = lax.all_gather(w_up, "sp", axis=0, tiled=True)
    down_full = lax.all_gather(w_down, "sp", axis=0, tiled=True)

    core = lax.axis_index("tp") % 2
    first_row = lax.axis_index("sp") * ROWS
    angle = angles((first_row + jnp.arange(ROWS, dtype=jnp.int32)).astype(jnp.float32), ROPE)
    cosine, sine_part = jnp.cos(angle), jnp.sin(angle)
    rope_query = rotate(
        query_rope.astype(jnp.float32).reshape(ROWS, 2, ROPE), cosine[:, None, :], sine_part[:, None, :]
    ).astype(jnp.bfloat16).reshape(ROWS, 2 * ROPE)

    def my_half(array):
        return lax.dynamic_slice_in_dim(array, core * HALF, HALF, 0)

    latent_normed = rms_scale(my_half(latent).astype(jnp.float32), latent_gain).astype(jnp.bfloat16)
    key_rotated = rotate(my_half(key_rope).astype(jnp.float32), my_half(cosine), my_half(sine_part)).astype(jnp.bfloat16)
    quarters = key_rotated.reshape(4, 128, ROPE)
    packed = jnp.concatenate([quarters[0], quarters[2], quarters[1], quarters[3]], axis=1)
    shard = jnp.concatenate([latent_normed, packed], axis=0)

    heads_all, w_out_all = attention_call(query_nope, rope_query, shard, w_key, w_value, w_out)
    attention_proj = jnp.einsum("gtv,gvd->td", heads_all, w_out_all, preferred_element_type=jnp.float32)
    stream = resid.astype(jnp.float32) + attention_proj
    normed = rms_scale(stream, mix_gain).astype(jnp.bfloat16)
    row_piece = lax.all_gather(normed, "tp", axis=0, tiled=True)
    gate_value = jnp.dot(row_piece, gate_full, preferred_element_type=jnp.float32)
    upward = jnp.dot(row_piece, up_full, preferred_element_type=jnp.float32)
    hidden = (jax.nn.silu(gate_value) * upward).astype(jnp.bfloat16)
    down_term = lax.dot_general(
        hidden, down_full, (((1,), (1,)), ((), ())), preferred_element_type=jnp.float32
    ).astype(jnp.bfloat16)
    mixer_out = lax.psum_scatter(down_term, "tp", scatter_dimension=0, tiled=True).astype(jnp.float32)
    return (stream + 0.5 * mixer_out).astype(jnp.bfloat16)


def solution(mesh):
    return jax.shard_map(
        on_device,
        mesh=mesh,
        in_specs=(
            P(("sp", "tp"), None),
            P("sp", "tp"),
            P("sp", "tp"),
            P("sp", None),
            P("sp", None),
            P(),
            P(None, "tp"),
            P(None, "tp"),
            P("tp", None),
            P(),
            P("sp", "tp"),
            P("sp", "tp"),
            P("sp", "tp"),
        ),
        out_specs=P(("sp", "tp"), None),
        check_vma=False,
    )
```

time: 641 us -> 317 us (0.49)
  waiting for transfers between devices: 459 us -> 175 us
  Pallas kernels: 0 us -> 94.8 us
  blocking collectives: 53.5 us -> 0 us
  matrix products: 54.1 us -> 24.6 us
  local copies, waits for them, and re-layouts: 29.3 us -> 1.24 us
  other arithmetic: 22.9 us -> 5.65 us
    all_gather x1, waiting for transfers between devices: 333 us -> 41.7 us  [on_device(): row_piece = lax.all_gather(normed, 'tp', axis=0, tiled=True)]
    pallas_call x0 -> x1, Pallas kernels: none -> 94.8 us  [attention_call(): pl.pallas_call(attention_kernel, out_shape=(jax.ShapeDtypeStruct((8, 128,...]
    all_to_all x1 -> x0, blocking collectives: 53.5 us -> none  [summed_on_arrival(): lax.all_to_all(tiles, axis, split_axis=0, concat_axis=0, tiled=True)]
    dot_general x7 -> x2, matrix products: 46.2 us -> 16.8 us  [the longest x1 12 us: on_device(): lax.dot_general(hidden, down_full, (((1,), (1,)), ((), ())), preferred_el...]
    slice x2 -> x0, local copies, waits for them, and re-layouts: 10.8 us -> none  [in_one_piece(): lax.slice_in_dim(filled, at, at + a.shape[along], axis=along)]
    dynamic_slice x8 -> x1, local copies, waits for them, and re-layouts: 10.2 us -> 0.01 us  [my_half(): return lax.dynamic_slice_in_dim(array, core * HALF, HALF, 0)]
    reduce_sum x2 -> x0, other arithmetic: 9.32 us -> none  [the longest x1 8.61 us: attend(): weight_sum = weight_sum * factor + jnp.sum(weights, axis=-1)]
    all_gather x2 -> x3, waiting for transfers between devices: 90.7 us -> 95.3 us  [the longest x1 52 us: on_device(): up_full = lax.all_gather(w_up, 'sp', axis=0, tiled=True)]
  transfers between devices with their start and end apart: 4 -> 5, of which waited for: 3 -> 4; matrix products, arithmetic and copies ran while one was open for 12% -> 5% of each run, Pallas kernels for 0% -> 30%
where the time goes in v1:
time: 317 us; the launch traced here: 315 us
  waiting for transfers between devices  175 us (55%)
  Pallas kernels  94.8 us (30%)
  matrix products  24.6 us (8%)
  between operations  13.4 us (4%)
  other arithmetic  5.65 us (2%)
    pallas_call x1, Pallas kernels, attention_call(): pl.pallas_call(attention_kernel, out_shape=(jax.ShapeDtypeStruct((8, 128,...  94.8 us
    all_gather x1, waiting for transfers between devices, on_device(): up_full = lax.all_gather(w_up, 'sp', axis=0, tiled=True)  52 us
    all_gather x1, waiting for transfers between devices, on_device(): down_full = lax.all_gather(w_down, 'sp', axis=0, tiled=True)  43.3 us
    all_gather x1, waiting for transfers between devices, on_device(): row_piece = lax.all_gather(normed, 'tp', axis=0, tiled=True)  41.7 us
    reduce_scatter x1, waiting for transfers between devices, on_device(): lax.psum_scatter(down_term, 'tp', scatter_dimension=0, tiled=True)  35.7 us
    dot_general x1, matrix products, on_device(): lax.dot_general(hidden, down_full, (((1,), (1,)), ((), ())), preferred_el...  12 us
    dot_general x1, matrix products, on_device(): jnp.dot(row_piece, gate_full, preferred_element_type=jnp.float32)  7.83 us
  transfers between devices with their start and end apart: 5, of which 4 were waited for; matrix products, arithmetic and copies ran while one was open for 5% of the time, Pallas kernels for 30%

profile of v1, /device:TPU:1, one launch (start us, length us, event | category | flops | bytes accessed | tf_op | source)
XLA Modules:
  0.0 314.7 jit_solution(17714776504159535260)
XLA Ops:
  6.5 0.7 all-gather.7.cloned.1.call-update
  7.3 0.0 all-gather.5.cloned.1.call-start
  7.3 0.1 copy-done
  7.4 0.1 copy.26
  7.6 1.9 multiply_cosine_fusion
  9.5 0.2 copy.22
  9.7 0.2 copy.23
  9.9 0.2 subtract_convert_fusion
  10.1 0.2 fusion.4
  10.3 0.1 copy.20
  10.5 0.1 subtract_convert_fusion.1
  10.6 0.2 copy.25.rope
  10.7 0.1 fusion.13
  10.9 0.1 fusion.6
  11.0 0.1 fusion.11.shard
  11.1 0.1 copy-done.1
  11.3 0.1 copy-done.2
  11.4 0.0 copy-done.4
  11.5 94.8 %attention.1 = (bf16[8,128,256]{2,1,0:T(8,128)(2,1)S(1)}, bf16[8,256,2048]{2,1,0:T(8,128)(2,1)}) custom-call(bf16[1024,256]{1,0:T(8,128)(2,1)S(1)} %copy-done.2, bf16[1024,128]{1,0:T(8,128)(2,1)S(1)} %copy.25.rope, bf16[640,256]{1,0:T(8,128)(2,1)S(1)} %fusion.11.shard, bf16[256,256]{1,0:T(8,128)(2,1)S(1)} %copy-done.3, bf16[256,256]{1,0:T(8,128)(2,1)S(1)} %copy-done.4, ...), custom_call_target="tpu_custom_call" | custom-call | flops 60000002048 | bytes 30000000 | tf_op jit(solution)/shard_map/attention/pallas_call | solution.py:411
  106.3 4.8 %multiply_reduce_fusion = (f32[128]{0:T(128)S(1)}, f32[128,2048]{1,0:T(8,128)S(1)}) fusion(bf16[8,128,256]{2,1,0:T(8,128)(2,1)S(1)} %get-tuple-element.7, bf16[8,256,2048]{2,1,0:T(8,128)(2,1)} %get-tuple-element.8, bf16[128,2048]{1,0:T(8,128)(2,1)S(1)} %copy-done.5), kind=kOutput, calls=%fused_computation.6 | convolution fusion | flops 1074790272 | bytes 10486272 | tf_op jit(solution)/shard_map/gtv,gvd->td/dot_general | solution.py:491
  111.1 1.0 multiply_convert_fusion.1
  112.0 0.0 all-gather.11.cloned.1.call-start
  112.1 0.7 all-gather.11.cloned.1.call-update
  112.8 0.5 all-gather.9.cloned.1.call-update
  113.3 0.2 reduce-scatter.2.cloned.1.call-start
  113.6 41.7 %all-gather.5.cloned.1.call-done = bf16[1024,2048]{1,0:T(8,128)(2,1)} async-done(((bf16[128,2048]{1,0:T(8,128)(2,1)}), bf16[1024,2048]{1,0:T(8,128)(2,1)}) %all-gather.5.cloned.1.call-update) | async-done | bytes 4194320 | tf_op jit(solution)/shard_map/all_gather | solution.py:494
  155.3 7.8 %fusion.16 = f32[1024,704]{0,1:T(8,128)} fusion(bf16[1024,2048]{1,0:T(8,128)(2,1)} %all-gather.5.cloned.1.call-done, bf16[2048,704]{0,1:T(8,128)(2,1)} %all-gather.7.cloned.1.call-done), kind=kOutput, calls=%fused_computation.44 | convolution fusion | flops 2952790016 | bytes 9961472 | tf_op jit(solution)/shard_map/dot_general | solution.py:495
  163.2 43.3 %all-gather.11.cloned.1.call-done = bf16[2048,704]{0,1:T(8,128)(2,1)} async-done(((bf16[128,704]{0,1:T(8,128)(2,1)}), bf16[2048,704]{0,1:T(8,128)(2,1)}) %all-gather.11.cloned.1.call-update) | async-done | bytes 2883600 | tf_op jit(solution)/shard_map/all_gather | solution.py:471
  206.4 52.0 %all-gather.9.cloned.1.call-done = bf16[2048,704]{0,1:T(8,128)(2,1)} async-done(((bf16[128,704]{0,1:T(8,128)(2,1)}), bf16[2048,704]{0,1:T(8,128)(2,1)}) %all-gather.9.cloned.1.call-update) | async-done | bytes 2883600 | tf_op jit(solution)/shard_map/all_gather | solution.py:470
  258.4 12.0 %convolution_convert_fusion = bf16[1024,2048]{1,0:T(8,128)(2,1)} fusion(bf16[2048,704]{0,1:T(8,128)(2,1)} %all-gather.11.cloned.1.call-done, f32[1024,704]{0,1:T(8,128)} %fusion.16, bf16[1024,2048]{1,0:T(8,128)(2,1)} %all-gather.5.cloned.1.call-done, bf16[2048,704]{0,1:T(8,128)(2,1)} %all-gather.9.cloned.1.call-done), kind=kOutput, calls=%fused_computation | convolution fusion | flops 5912002560 | bytes 17039360 | tf_op jit(solution)/shard_map/dot_general | solution.py:498
  270.5 35.7 %reduce-scatter.2.cloned.1.call-done = bf16[128,2048]{1,0:T(8,128)(2,1)} async-done(((bf16[1024,2048]{1,0:T(8,128)(2,1)}), bf16[128,2048]{1,0:T(8,128)(2,1)}) %reduce-scatter.2.cloned.1.call-update) | async-done | bytes 524304 | tf_op jit(solution)/shard_map/reduce_scatter | solution.py:501
  306.2 2.0 add_convert_fusion
  (29 shorter events, 0.3 us)
Async XLA Ops:
  6.5 0.9 copy-start
  6.5 3.5 %copy-start.6 = (bf16[1024,256]{1,0:T(8,128)(2,1)S(1)}, bf16[1024,256]{1,0:T(8,128)(2,1)}, u32[]{:S(2)}) copy-start(bf16[1024,256]{1,0:T(8,128)(2,1)} %param.16) | copy-start | bytes 1572868
  6.5 3.7 %copy-start.7 = (bf16[1024,128]{1,0:T(8,128)(2,1)S(1)}, bf16[1024,128]{1,0:T(8,128)(2,1)}, u32[]{:S(2)}) copy-start(bf16[1024,128]{1,0:T(8,128)(2,1)} %param.15) | copy-start | bytes 786436
  6.5 107.1 %all-gather.7.cloned.1.call-start = ((), (), s32[]{:S(2)}) async-start(), calls=%async_computation.2 | async-start | bytes 3063808 | tf_op jit(solution)/shard_map/all_gather | solution.py:469
  7.3 148.1 %all-gather.5.cloned.1.call-start = ((), (), s32[]{:S(2)}) async-start(), calls=%async_computation.1 | async-start | bytes 4718592 | tf_op jit(solution)/shard_map/all_gather | solution.py:494
  9.7 1.2 copy-start.9
  10.0 1.2 copy-start.1
  10.0 1.3 copy-start.2
  10.1 1.4 copy-start.3
  10.1 1.4 copy-start.4
  11.5 94.8 %copy-start.5 = (bf16[128,2048]{1,0:T(8,128)(2,1)S(1)}, bf16[128,2048]{1,0:T(8,128)(2,1)}, u32[]{:S(2)}) copy-start(bf16[128,2048]{1,0:T(8,128)(2,1)} %param.13) | copy-start | bytes 1572868
  106.2 4.8 %copy-start.8 = (f32[2048]{0:T(1024)S(1)}, f32[2048]{0:T(1024)}, u32[]{:S(2)}) copy-start(f32[2048]{0:T(1024)} %param.22) | copy-start | bytes 24580
  112.0 94.4 %all-gather.11.cloned.1.call-start = ((), (), s32[]{:S(2)}) async-start(), calls=%async_computation.4 | async-start | bytes 3063808 | tf_op jit(solution)/shard_map/all_gather | solution.py:471
  112.8 145.7 %all-gather.9.cloned.1.call-start = ((), (), s32[]{:S(2)}) async-start(), calls=%async_computation.3 | async-start | bytes 3063808 | tf_op jit(solution)/shard_map/all_gather | solution.py:470
  113.3 192.9 %reduce-scatter.2.cloned.1.call-start = ((), (), s32[]{:S(2)}) async-start(), calls=%async_computation.5 | async-start | bytes 4718592 | tf_op jit(solution)/shard_map/reduce_scatter | solution.py:501
Sparse Core Ops, SparseCore 0:
  9.4 65.9 all-gather.6
  112.2 43.1 all-gather.4
  157.5 48.9 all-gather.10
  208.4 49.9 all-gather.8
  270.6 35.5 reduce-scatter.1

commit v2 on v1

--- a/solution.py
+++ b/solution.py
@@ -65,11 +65,13 @@
     return found
 
 
-def attention_kernel(
-    nope, rope, shard, w_key, w_value, w_out, heads_all, w_out_all,
+def layer_kernel(
+    nope, rope, shard, w_key, w_value, w_out, mixer, resid, mix_gain, result,
     lat, far_nope, far_rope, queries, keys, values_t, w_value_t, top, total, acc, head_out,
+    heads_all, w_out_all, weights_all, stream, rows_all, halves, got, summed, relay, arrived,
     send_sem, recv_sem, pair_send, pair_recv, query_send, query_recv, head_send, head_recv,
-    out_send, out_recv, local_sem,
+    out_send, out_recv, local_sem, mixer_send, mixer_recv, row_send, row_recv, part_send, part_recv,
+    sum_send, sum_recv,
 ):
     s = lax.axis_index("sp")
     t = lax.axis_index("tp")
@@ -110,38 +112,41 @@
 
     own = 2 * s + core
 
-    def relative(pair, plane):
-        return 2 * sp_at(*pair) + plane
-
-    def shard_copy(phase, index):
-        source, (first, count), step, slot = SENDS[phase][index]
+    def piece(kind, block, rows):
+        first, count = rows
+        if kind == 0:
+            return lat.at[2 * block + core, pl.ds(first, count)]
+        return weights_all.at[pl.ds(128 * block + first // 5, count // 5)]
+
+    def shard_copy(kind, phase, index):
+        source, rows, step, slot = SENDS[phase][index]
         number = sum(len(one) for one in SENDS[:phase]) + index
         place = at_receiver(source, step)
-        block = relative(source, core)
-        if phase == 0:
-            source_ref = shard
+        there = piece(kind, sp_at(*source), rows)
+        if phase > 0:
+            here = there
         else:
-            source_ref = lat.at[block, pl.ds(first, count)]
+            here = shard if kind == 0 else mixer
         return pltpu.make_async_remote_copy(
-            source_ref, lat.at[block, pl.ds(first, count)],
-            send_sem.at[number], recv_sem.at[4 * place + slot],
+            here, there,
+            (send_sem, mixer_send)[kind].at[number], (recv_sem, mixer_recv)[kind].at[4 * place + slot],
             device_id=(sp_at(*step), t), device_id_type=MESH)
 
-    def start_phase(phase):
+    def start_phase(kind, phase):
         for index in range(len(SENDS[phase])):
-            shard_copy(phase, index).start()
-
-    def wait_received(phase):
-        for index, (source, (first, count), step, slot) in enumerate(SENDS[phase]):
+            shard_copy(kind, phase, index).start()
+
+    def wait_received(kind, phase, first_index=0, last_index=12):
+        for source, rows, step, slot in SENDS[phase][first_index:last_index]:
             place = at_receiver(source, step)
-            block = relative(ORDER[place], core)
+            there = piece(kind, sp_at(*ORDER[place]), rows)
             pltpu.make_async_remote_copy(
-                lat.at[block, pl.ds(first, count)], lat.at[block, pl.ds(first, count)],
-                send_sem.at[0], recv_sem.at[4 * place + slot],
+                there, there,
+                (send_sem, mixer_send)[kind].at[0], (recv_sem, mixer_recv)[kind].at[4 * place + slot],
                 device_id=(sp_at(*step), t), device_id_type=MESH).wait_recv()
 
     def pair_copy(place):
-        block = relative(ORDER[place], core)
+        block = 2 * sp_at(*ORDER[place]) + core
         return pltpu.make_async_remote_copy(
             shard if place == 0 else lat.at[block], lat.at[block],
             pair_send.at[place], pair_recv.at[place],
@@ -179,7 +184,7 @@
             out_send.at[number], out_recv.at[number],
             device_id=(s, partner), device_id_type=MESH).wait_recv()
 
-    start_phase(0)
+    start_phase(0, 0)
     pair_copy(0).start()
     for number in range(3):
         out_copy(*out_sends[number]).start()
@@ -187,6 +192,8 @@
     own_shard.start()
     own_out = pltpu.make_async_copy(w_out, w_out_all.at[t], local_sem.at[1])
     own_out.start()
+    own_mixer = pltpu.make_async_copy(mixer, weights_all.at[pl.ds(128 * s, 128)], local_sem.at[3])
+    own_mixer.start()
 
     w_value_t[...] = jnp.transpose(w_value[...].astype(jnp.float32)).astype(jnp.bfloat16)
     top[...] = jnp.full_like(top, masked_score)
@@ -274,22 +281,23 @@
     def advance(place, carry):
         @pl.when(place == 1)
         def _():
-            wait_received(0)
-            start_phase(1)
+            wait_received(0, 0)
+            start_phase(0, 1)
             for at in (1, 2, 3, 4):
                 pair_copy(at).start()
+            start_phase(1, 0)
 
         @pl.when(place == 3)
         def _():
-            wait_some(1, 0, 4)
-            start_phase(2)
+            wait_received(0, 1, 0, 4)
+            start_phase(0, 2)
             for at in (5, 6):
                 pair_copy(at).start()
 
         @pl.when(place == 5)
         def _():
-            wait_some(1, 4, 12)
-            start_phase(3)
+            wait_received(0, 1, 4, 12)
+            start_phase(0, 3)
             for at in (7, 8, 9, 10):
                 pair_copy(at).start()
 
@@ -302,19 +310,23 @@
 
         @pl.when(place == 8)
         def _():
-            wait_received(2)
-            wait_received(3)
-            start_phase(4)
+            wait_received(0, 2)
+            wait_received(0, 3)
+            start_phase(0, 4)
             for at in (11, 12, 13, 14):
                 pair_copy(at).start()
-
-        @pl.when(place == 13)
-        def _():
-            wait_received(4)
+            wait_received(1, 0)
+            start_phase(1, 1)
+
+        @pl.when(place == 12)
+        def _():
+            wait_received(0, 4)
             pair_copy(15).start()
             out_wait(3)
             out_wait(4)
             out_copy(*out_sends[7]).start()
+            wait_received(1, 1, 0, 4)
+            start_phase(1, 2)
 
         dy = pick(place, [pair[0] for pair in ORDER])
         dz = pick(place, [pair[1] for pair in ORDER])
@@ -334,15 +346,6 @@
 
         lax.fori_loop(0, 2, plane, 0)
         return carry
-
-    def wait_some(phase, first_index, last_index):
-        for source, (first, count), step, slot in SENDS[phase][first_index:last_index]:
-            place = at_receiver(source, step)
-            block = relative(ORDER[place], core)
-            pltpu.make_async_remote_copy(
-                lat.at[block, pl.ds(first, count)], lat.at[block, pl.ds(first, count)],
-                send_sem.at[0], recv_sem.at[4 * place + slot],
-                device_id=(sp_at(*step), t), device_id_type=MESH).wait_recv()
 
     lax.fori_loop(0, 16, advance, 0)
 
@@ -372,6 +375,9 @@
         mine.start()
         mine.wait()
 
+    wait_received(1, 1, 4, 12)
+    start_phase(1, 3)
+
     def head_wait(slot, carry):
         @pl.when((t >= 4) | (slot != t))
         def _():
@@ -381,41 +387,178 @@
 
         return carry
 
-    lax.fori_loop(0, 8, head_wait, 0)
-
     own_out.wait()
     for number in (2, 5, 6, 7):
         out_wait(number)
+    lax.fori_loop(0, 8, head_wait, 0)
+
+    stream[...] = resid[...].astype(jnp.float32)
+
+    def project(slot, carry):
+        stream[...] += jnp.dot(heads_all[slot], w_out_all[slot], preferred_element_type=jnp.float32)
+        return carry
+
+    lax.fori_loop(0, 8, project, 0)
+    rows_f32 = stream[...]
+    scale = lax.rsqrt(jnp.mean(rows_f32 * rows_f32, axis=-1, keepdims=True) + norm_eps)
+    rows_all[t] = (rows_f32 * scale * mix_gain[...]).astype(jnp.bfloat16)
+
+    high, low = (0, 64), (64, 64)
+    all_rows = (0, 128)
+    row_sends = (
+        (0, t, all_rows, right), (1, t, all_rows, left), (2, t, all_rows, partner),
+        (3, right, high, left), (4, left, low, right),
+        (5, right, all_rows, partner), (6, left, all_rows, partner), (7, across, all_rows, partner),
+    )
+    row_receives = (
+        (0, left, all_rows), (1, right, all_rows), (2, partner, all_rows),
+        (3, across, high), (4, across, low),
+        (5, other(right), all_rows), (6, other(left), all_rows), (7, other(across), all_rows),
+    )
+
+    def row_copy(number):
+        _, slot, (first, count), target = row_sends[number]
+        here = rows_all.at[slot, pl.ds(first, count)]
+        return pltpu.make_async_remote_copy(
+            here, here, row_send.at[number], row_recv.at[number],
+            device_id=(s, target), device_id_type=MESH)
+
+    def row_wait(number):
+        _, slot, (first, count) = row_receives[number]
+        here = rows_all.at[slot, pl.ds(first, count)]
+        pltpu.make_async_remote_copy(
+            here, here, row_send.at[number], row_recv.at[number],
+            device_id=(s, partner), device_id_type=MESH).wait_recv()
+
+    for number in range(3):
+        row_copy(number).start()
+
+    wait_received(1, 2)
+    wait_received(1, 3)
+    start_phase(1, 4)
+    own_mixer.wait()
+    row_wait(0)
+    row_wait(1)
+    for number in (3, 4, 5, 6):
+        row_copy(number).start()
+    wait_received(1, 4)
+
+    def part_copy(step):
+        return pltpu.make_async_remote_copy(
+            halves.at[step, 1 - core], got.at[step], part_send.at[step], part_recv.at[step],
+            device_id=(s, partner), device_id_type=MESH)
+
+    def chip_total(step):
+        part_copy(step).wait_recv()
+        return halves[step, core].astype(jnp.float32) + got[step].astype(jnp.float32)
+
+    def sum_copy(number):
+        here, there, target = (
+            (summed.at[1], arrived.at[0], right),
+            (summed.at[2], arrived.at[1], left),
+            (summed.at[3, pl.ds(0, 64)], relay.at[0], right),
+            (summed.at[3, pl.ds(64, 64)], relay.at[1], left),
+            (relay.at[0], arrived.at[2, pl.ds(0, 64)], right),
+            (relay.at[1], arrived.at[2, pl.ds(64, 64)], left),
+        )[number]
+        return pltpu.make_async_remote_copy(
+            here, there, sum_send.at[number], sum_recv.at[number],
+            device_id=(s, target), device_id_type=MESH)
+
+    def mix(step, carry):
+        @pl.when(step == 0)
+        def _():
+            row_wait(2)
+
+        @pl.when(step == 1)
+        def _():
+            row_wait(5)
+            row_wait(6)
+
+        @pl.when(step == 2)
+        def _():
+            row_wait(3)
+            row_wait(4)
+            row_copy(7).start()
+
+        @pl.when(step == 3)
+        def _():
+            row_wait(7)
+
+        chip = (x + pick(step, (0, 1, 3, 2))) % SIDE
+        rows = rows_all[pl.ds(2 * chip, 2)].reshape(256, 2048)
+        both = jnp.dot(rows, weights_all[:, 0:1408], preferred_element_type=jnp.float32)
+        gate_value, upward = both[:, 0:704], both[:, 704:1408]
+        hidden = (gate_value / (1.0 + jnp.exp(-gate_value)) * upward).astype(jnp.bfloat16)
+        down = lax.dot_general(
+            hidden, weights_all[:, 1408:2112], (((1,), (1,)), ((), ())), preferred_element_type=jnp.float32)
+        halves[step] = down.astype(jnp.bfloat16).reshape(2, 128, 2048)
+        part_copy(step).start()
+
+        @pl.when(step == 1)
+        def _():
+            stream[...] += 0.5 * chip_total(0)
+
+        @pl.when(step == 2)
+        def _():
+            summed[1] = chip_total(1).astype(jnp.bfloat16)
+            sum_copy(0).start()
+
+        @pl.when(step == 3)
+        def _():
+            summed[2] = chip_total(2).astype(jnp.bfloat16)
+            sum_copy(1).start()
+
+        return carry
+
+    lax.fori_loop(0, 4, mix, 0)
+    summed[3] = chip_total(3).astype(jnp.bfloat16)
+    sum_copy(2).start()
+    sum_copy(3).start()
+    sum_copy(2).wait_recv()
+    sum_copy(4).start()
+    sum_copy(3).wait_recv()
+    sum_copy(5).start()
+    sum_copy(0).wait_recv()
+    sum_copy(1).wait_recv()
+    stream[...] += 0.5 * (arrived[0].astype(jnp.float32) + arrived[1].astype(jnp.float32))
+    sum_copy(4).wait_recv()
+    sum_copy(5).wait_recv()
+    result[...] = (stream[...] + 0.5 * arrived[2].astype(jnp.float32)).astype(jnp.bfloat16)
+
+    for number in range(6):
+        sum_copy(number).wait_send()
+    for step in range(4):
+        part_copy(step).wait_send()
     for number in range(8):
+        row_copy(number).wait_send()
         out_copy(*out_sends[number]).wait_send()
     for copy in query_copies():
         copy.wait_send()
     for phase in range(len(SENDS)):
         for index in range(len(SENDS[phase])):
-            shard_copy(phase, index).wait_send()
+            shard_copy(0, phase, index).wait_send()
+            shard_copy(1, phase, index).wait_send()
     for place in range(16):
         pair_copy(place).wait_send()
-    for part in range(4):
-        head_copy(1, part).wait_send()
-
-        @pl.when(t != part)
-        def _():
-            head_copy(0, part).wait_send()
-
-
-def attention_call(nope, rope, shard, w_key, w_value, w_out):
+    for number in range(4):
+        head_copy(1, number).wait_send()
+
+        @pl.when(t != number)
+        def _():
+            head_copy(0, number).wait_send()
+
+
+def layer_call(nope, rope, shard, w_key, w_value, w_out, mixer, resid, mix_gain):
     vmem = pl.BlockSpec(memory_space=pltpu.VMEM)
     anywhere = pl.BlockSpec(memory_space=pl.ANY)
     dma = pltpu.SemaphoreType.DMA
     bf16, f32 = jnp.bfloat16, jnp.float32
     return pl.pallas_call(
-        attention_kernel,
-        out_shape=(
-            jax.ShapeDtypeStruct((8, 128, 256), bf16),
-            jax.ShapeDtypeStruct((8, 256, 2048), bf16),
-        ),
-        in_specs=[vmem] * 5 + [anywhere],
-        out_specs=[anywhere, anywhere],
+        layer_kernel,
+        out_shape=jax.ShapeDtypeStruct((128, 2048), bf16),
+        in_specs=[vmem] * 5 + [anywhere, anywhere, vmem, vmem],
+        out_specs=vmem,
         scratch_shapes=[
             pltpu.VMEM((32, SHARD, 256), bf16),
             pltpu.VMEM((HALF, 256), bf16),
@@ -428,14 +571,25 @@
             pltpu.VMEM((2, 2, 1, HALF), f32),
             pltpu.VMEM((2, 2, VDIM, HALF), f32),
             pltpu.VMEM((2, HALF, 256), bf16),
+            pltpu.VMEM((8, 128, 256), bf16),
+            pltpu.VMEM((8, 256, 2048), bf16),
+            pltpu.VMEM((2048, 2112), bf16),
+            pltpu.VMEM((128, 2048), f32),
+            pltpu.VMEM((8, 128, 2048), bf16),
+            pltpu.VMEM((4, 2, 128, 2048), bf16),
+            pltpu.VMEM((4, 128, 2048), bf16),
+            pltpu.VMEM((4, 128, 2048), bf16),
+            pltpu.VMEM((2, 64, 2048), bf16),
+            pltpu.VMEM((3, 128, 2048), bf16),
             dma((32,)), dma((64,)), dma((16,)), dma((16,)), dma((2,)), dma((2,)), dma((8,)), dma((8,)),
-            dma((8,)), dma((8,)), dma((3,)),
+            dma((8,)), dma((8,)), dma((4,)),
+            dma((32,)), dma((64,)), dma((8,)), dma((8,)), dma((4,)), dma((4,)), dma((6,)), dma((6,)),
         ],
         compiler_params=pltpu.CompilerParams(
-            collective_id=0, has_side_effects=True, vmem_limit_bytes=48 * 1024 * 1024),
+            collective_id=0, has_side_effects=True, vmem_limit_bytes=67_000_000),
         cost_estimate=pl.CostEstimate(flops=60_000_000_000, bytes_accessed=30_000_000, transcendentals=18_000_000),
-        name="attention",
-    )(nope, rope, shard, w_key, w_value, w_out)
+        name="layer",
+    )(nope, rope, shard, w_key, w_value, w_out, mixer, resid, mix_gain)
 
 
 def rotate(values_in, cosine, sine_part):
@@ -466,10 +620,6 @@
     resid, query_nope, query_rope, latent, key_rope, latent_gain, w_key, w_value, w_out, mix_gain,
     w_gate, w_up, w_down,
 ):
-    gate_full = lax.all_gather(w_gate, "sp", axis=0, tiled=True)
-    up_full = lax.all_gather(w_up, "sp", axis=0, tiled=True)
-    down_full = lax.all_gather(w_down, "sp", axis=0, tiled=True)
-
     core = lax.axis_index("tp") % 2
     first_row = lax.axis_index("sp") * ROWS
     angle = angles((first_row + jnp.arange(ROWS, dtype=jnp.int32)).astype(jnp.float32), ROPE)
@@ -487,19 +637,9 @@
     packed = jnp.concatenate([quarters[0], quarters[2], quarters[1], quarters[3]], axis=1)
     shard = jnp.concatenate([latent_normed, packed], axis=0)
 
-    heads_all, w_out_all = attention_call(query_nope, rope_query, shard, w_key, w_value, w_out)
-    attention_proj = jnp.einsum("gtv,gvd->td", heads_all, w_out_all, preferred_element_type=jnp.float32)
-    stream = resid.astype(jnp.float32) + attention_proj
-    normed = rms_scale(stream, mix_gain).astype(jnp.bfloat16)
-    row_piece = lax.all_gather(normed, "tp", axis=0, tiled=True)
-    gate_value = jnp.dot(row_piece, gate_full, preferred_element_type=jnp.float32)
-    upward = jnp.dot(row_piece, up_full, preferred_element_type=jnp.float32)
-    hidden = (jax.nn.silu(gate_value) * upward).astype(jnp.bfloat16)
-    down_term = lax.dot_general(
-        hidden, down_full, (((1,), (1,)), ((), ())), preferred_element_type=jnp.float32
-    ).astype(jnp.bfloat16)
-    mixer_out = lax.psum_scatter(down_term, "tp", scatter_dimension=0, tiled=True).astype(jnp.float32)
-    return (stream + 0.5 * mixer_out).astype(jnp.bfloat16)
+    mixer = jnp.concatenate([w_gate, w_up, w_down], axis=1)
+    return layer_call(
+        query_nope, rope_query, shard, w_key, w_value, w_out, mixer, resid, mix_gain.reshape(1, -1))
 
 
 def solution(mesh):

time: 317 us -> 180 us (0.57)
  the two profiles are of different devices: /device:TPU:1 before, /device:TPU:58 now
where the time goes in v2:
time: 180 us
  Pallas kernels  166 us (92%)
  local copies, waits for them, and re-layouts  9.49 us (5%)
  other arithmetic  3.43 us (2%)
    pallas_call x1, Pallas kernels, layer_call(): pl.pallas_call(layer_kernel, out_shape=jax.ShapeDtypeStruct((128, 2048),...  166 us
    unnamed x18, local copies, waits for them, and re-layouts  6.41 us

profile of v2, /device:TPU:58, one launch (start us, length us, event | category | flops | bytes accessed | tf_op | source)
XLA Modules:
  0.0 179.5 jit_solution(15977103953596072370)
XLA Ops:
  0.0 0.8 constant_dynamic-slice_fusion
  0.8 0.1 copy.35
  1.0 1.9 %multiply_cosine_fusion = (f32[1024,32]{1,0:T(8,128)S(1)}, f32[1024,32]{1,0:T(8,128)S(1)}) fusion(f32[1024]{0:T(1024)S(1)} %add_convert_fusion.2, f32[32]{0:T(128)S(1)} %multiply_power_fusion), kind=kLoop, calls=%fused_computation.1 | loop fusion | flops 32768 | bytes 266368 | tf_op jit(solution)/shard_map/cos | solution.py:626
  2.9 0.0 copy-start
  2.9 0.1 subtract_convert_fusion
  3.1 0.1 fusion.12
  3.2 0.8 copy-done
  4.0 0.1 fusion.3
  4.1 0.0 copy-start.5
  4.1 0.7 copy-done.5
  4.8 0.1 fusion.5
  4.9 0.8 fusion.10.shard
  5.8 0.2 copy.28
  5.9 0.0 copy-start.1
  5.9 0.2 copy.29
  6.1 0.8 copy-done.1
  6.9 0.1 copy.26
  7.1 0.1 subtract_convert_fusion.1
  7.2 0.0 copy-start.2
  7.2 0.8 copy.34.rope
  8.1 0.1 copy-done.2
  8.1 0.0 copy-start.3
  8.1 0.1 copy.31
  8.3 0.8 copy-done.3
  9.1 0.0 copy-start.4
  9.1 0.1 copy.32
  9.2 0.8 copy-done.4
  10.0 0.1 copy.33
  10.1 1.1 concatenate.21.mixer
  11.2 166.4 %layer.1 = bf16[128,2048]{1,0:T(8,128)(2,1)} custom-call(bf16[1024,256]{1,0:T(8,128)(2,1)} %nope.1, bf16[1024,128]{1,0:T(8,128)(2,1)} %copy.34.rope, bf16[640,256]{1,0:T(8,128)(2,1)} %fusion.10.shard, bf16[256,256]{1,0:T(8,128)(2,1)} %w_key.1, bf16[256,256]{1,0:T(8,128)(2,1)} %w_value.1, bf16[256,2048]{1,0:T(8,128)(2,1)} %w_out.1, ...), custom_call_target="tpu_custom_call" | custom-call | flops 60000002048 | bytes 30000000 | tf_op jit(solution)/shard_map/layer/pallas_call | solution.py:557
  177.6 1.9 %copy.37 = bf16[128,2048]{1,0:T(8,128)(2,1)} copy(bf16[128,2048]{1,0:T(8,128)(2,1)} %layer.1) | data formatting | bytes 1048576
  (6 shorter events, 0.1 us)
Async XLA Ops:
  2.9 1.0 copy-start
  4.1 0.7 copy-start.5
  5.9 1.0 copy-start.1
  7.2 0.9 copy-start.2
  8.1 0.9 copy-start.3
  9.1 0.9 copy-start.4

commit v3 on v2

v3 whole, which is shorter than its diff:
```python
import functools

import jax
import jax.numpy as jnp
import numpy as np
from jax import lax
from jax.experimental import pallas as pl
from jax.experimental.pallas import tpu as pltpu
from jax.sharding import PartitionSpec as P

NOPE = 128
ROPE = 64
VDIM = 128
ROWS = 1024
HALF = 512
SIDE = 4
QUARTER = 256
UNITS = 704
SHARD = QUARTER + QUARTER // 4

norm_eps = 1e-06
masked_score = -1e30
theta_base = 10000.0
score_base2 = (NOPE + ROPE) ** (-0.5) * 1.4426950408889634
MESH = pl.DeviceIdType.MESH

ORDER = ((0, 0), (1, 0), (3, 0), (0, 1), (0, 3), (2, 0), (0, 2), (1, 1), (1, 3), (3, 1), (3, 3),
         (2, 1), (2, 3), (1, 2), (3, 2), (2, 2))
PLACE = {pair: p for p, pair in enumerate(ORDER)}
ALPHA, BETA, FULL = (0, 320), (320, 320), (0, 640)
ALPHA0, ALPHA1, BETA0, BETA1 = (0, 160), (160, 160), (320, 160), (480, 160)

SENDS = (
    (((0, 0), FULL, (1, 0), 0), ((0, 0), FULL, (-1, 0), 0), ((0, 0), FULL, (0, 1), 0), ((0, 0), FULL, (0, -1), 0)),
    (
        ((1, 0), ALPHA, (-1, 0), 0), ((3, 0), BETA, (1, 0), 1),
        ((0, 1), ALPHA, (0, -1), 0), ((0, 3), BETA, (0, 1), 1),
        ((1, 0), ALPHA, (0, 1), 0), ((1, 0), ALPHA, (0, -1), 0),
        ((3, 0), ALPHA, (0, 1), 0), ((3, 0), ALPHA, (0, -1), 0),
        ((0, 1), BETA, (1, 0), 1), ((0, 1), BETA, (-1, 0), 1),
        ((0, 3), BETA, (1, 0), 1), ((0, 3), BETA, (-1, 0), 1),
    ),
    (
        ((2, 0), ALPHA, (0, 1), 0), ((2, 0), ALPHA, (0, -1), 0),
        ((0, 2), BETA, (1, 0), 1), ((0, 2), BETA, (-1, 0), 1),
    ),
    (
        ((1, 1), ALPHA0, (0, -1), 0), ((1, 3), ALPHA1, (0, 1), 2),
        ((3, 1), ALPHA0, (0, -1), 0), ((3, 3), ALPHA1, (0, 1), 2),
        ((1, 1), BETA0, (-1, 0), 1), ((3, 1), BETA1, (1, 0), 2),
        ((1, 3), BETA0, (-1, 0), 1), ((3, 3), BETA1, (1, 0), 2),
    ),
    (
        ((2, 1), ALPHA0, (0, -1), 0), ((2, 3), ALPHA1, (0, 1), 1),
        ((1, 2), BETA0, (-1, 0), 2), ((3, 2), BETA1, (1, 0), 3),
    ),
)


def at_receiver(source, step):
    return PLACE[((source[0] - step[0]) % SIDE, (source[1] - step[1]) % SIDE)]


def pick(index, values):
    found = jnp.int32(values[0])
    for at in range(1, len(values)):
        found = jnp.where(index == at, jnp.int32(values[at]), found)
    return found


def layer_kernel(
    nope_in, rope_in, latent_in, key_in, gain_in, w_key_in, w_value_in, w_out, resid_in, mix_gain_in,
    gate_in, up_in, down_in, row_cos_in, row_sin_in, block_cos_in, block_sin_in, result,
    nope, rope, latent, key_rope, gain, w_key, w_value, resid, mix_gain,
    row_cos, row_sin, block_cos, block_sin, turned_queries,
    lat, far_nope, far_rope, queries, keys, values_t, held, w_value_t, top, total, acc, head_out,
    heads_all, w_out_all, weights_all, hidden, stream, rows_all, halves, got, summed, relay, arrived,
    send_sem, recv_sem, side_send, side_recv, pair_send, pair_recv, query_send, query_recv, head_send, head_recv,
    out_send, out_recv, local_sem, mixer_send, mixer_recv, row_send, row_recv, part_send, part_recv,
    sum_send, sum_recv, load_sem,
):
    s = lax.axis_index("sp")
    t = lax.axis_index("tp")
    z, y = s // SIDE, s % SIDE
    x, core = t // 2, t % 2
    mirror = 15 - s

    def sp_at(dy, dz):
        return ((z + dz + SIDE) % SIDE) * SIDE + (y + dy + SIDE) % SIDE

    def tp_at(dx):
        return ((x + dx + SIDE) % SIDE) * 2 + core

    partner = x * 2 + 1 - core
    mine = 2 * (x % 2) + core
    beside = 2 * (1 - x % 2) + core

    barrier = pltpu.get_barrier_semaphore()
    for step in (1, 2, 3):
        pl.semaphore_signal(barrier, inc=1, device_id=(sp_at(step, 0), t), device_id_type=MESH)
        pl.semaphore_signal(barrier, inc=1, device_id=(sp_at(0, step), t), device_id_type=MESH)
    for step in range(1, 8):
        pl.semaphore_signal(barrier, inc=1, device_id=(s, (t + step) % 8), device_id_type=MESH)
    for step in range(8):
        pl.semaphore_signal(barrier, inc=1, device_id=(mirror, (t + step) % 8), device_id_type=MESH)

    quarter_rows = pl.ds(pl.multiple_of((2 * (x % 2) + core) * QUARTER, QUARTER), QUARTER)
    loads = [
        pltpu.make_async_copy(source, target, load_sem.at[number])
        for number, (source, target) in enumerate((
            (latent_in.at[quarter_rows], latent), (key_in.at[:, quarter_rows], key_rope), (gain_in, gain),
            (block_cos_in, block_cos), (block_sin_in, block_sin), (row_cos_in, row_cos), (row_sin_in, row_sin),
            (rope_in, rope), (nope_in, nope), (w_value_in, w_value), (w_key_in, w_key),
            (gate_in, weights_all.at[s, pl.ds(0, UNITS)]), (up_in, weights_all.at[s, pl.ds(UNITS, UNITS)]),
            (down_in, weights_all.at[s, pl.ds(2 * UNITS, UNITS)]), (resid_in, resid), (mix_gain_in, mix_gain),
        ))
    ]
    for load in loads:
        load.start()

    def rotated(rows_in, first):
        count = rows_in.shape[0]
        at = pl.ds(first, count)
        near_cos, near_sin = row_cos[at, :], row_sin[at, :]
        far_cos, far_sin = block_cos[pl.ds(s, 1), :], block_sin[pl.ds(s, 1), :]
        cosine = far_cos * near_cos - far_sin * near_sin
        sine = far_sin * near_cos + far_cos * near_sin
        lane = lax.broadcasted_iota(jnp.int32, rows_in.shape, 1) % ROPE
        swapped = jnp.where(lane < ROPE // 2, -pltpu.roll(rows_in, 96, 1), pltpu.roll(rows_in, 32, 1))
        return rows_in * cosine + swapped * sine

    own = 4 * s + 2 * (x % 2) + core
    for load in loads[:7]:
        load.wait()
    wide = latent[...].astype(jnp.float32)
    scale = lax.rsqrt(jnp.mean(wide * wide, axis=-1, keepdims=True) + norm_eps)
    lat[own, pl.ds(0, QUARTER), :] = (wide * scale * gain[...]).astype(jnp.bfloat16)
    once = key_rope[...].astype(jnp.float32)
    twice = rotated(jnp.transpose(jnp.concatenate([once, once], axis=0)), (2 * (x % 2) + core) * QUARTER).astype(jnp.bfloat16)
    front_lanes = lax.broadcasted_iota(jnp.int32, (64, 128), 1) < ROPE
    for side in range(2):
        lat[own, pl.ds(QUARTER, 64), side * 128:(side + 1) * 128] = jnp.where(
            front_lanes, twice[64 * side:64 * side + 64], twice[128 + 64 * side:192 + 64 * side])
    for load in loads[7:9]:
        load.wait()
    for first in (HALF, 0):
        turned_queries[pl.ds(first, HALF), :] = rotated(
            rope[pl.ds(first, HALF), :].astype(jnp.float32), first).astype(jnp.bfloat16)
    for load in loads[9:]:
        load.wait()
    pl.semaphore_wait(barrier, 21)

    def query_copies():
        return (
            pltpu.make_async_remote_copy(
                nope.at[pl.ds(HALF, HALF)], far_nope, query_send.at[0], query_recv.at[0],
                device_id=(mirror, t), device_id_type=MESH),
            pltpu.make_async_remote_copy(
                turned_queries.at[pl.ds(HALF, HALF)], far_rope, query_send.at[1], query_recv.at[1],
                device_id=(mirror, t), device_id_type=MESH),
        )

    def piece(kind, block, rows):
        first, count = rows
        if kind == 0:
            return lat.at[4 * block + mine, pl.ds(first // 2, count // 2)]
        return weights_all.at[block, pl.ds(first * 33 // 10, count * 33 // 10)]

    def shard_copy(kind, phase, index):
        source, rows, step, slot = SENDS[phase][index]
        number = sum(len(one) for one in SENDS[:phase]) + index
        place = at_receiver(source, step)
        there = piece(kind, sp_at(*source), rows)
        return pltpu.make_async_remote_copy(
            there, there,
            (send_sem, mixer_send)[kind].at[number], (recv_sem, mixer_recv)[kind].at[4 * place + slot],
            device_id=(sp_at(*step), t), device_id_type=MESH)

    def start_phase(kind, phase):
        for index in range(len(SENDS[phase])):
            shard_copy(kind, phase, index).start()

    def wait_received(kind, phase, first_index=0, last_index=12):
        for source, rows, step, slot in SENDS[phase][first_index:last_index]:
            place = at_receiver(source, step)
            there = piece(kind, sp_at(*ORDER[place]), rows)
            pltpu.make_async_remote_copy(
                there, there,
                (send_sem, mixer_send)[kind].at[0], (recv_sem, mixer_recv)[kind].at[4 * place + slot],
                device_id=(sp_at(*step), t), device_id_type=MESH).wait_recv()

    def pair_copy(place, quarter, number):
        there = lat.at[4 * sp_at(*ORDER[place]) + quarter]
        return pltpu.make_async_remote_copy(
            there, there, pair_send.at[number], pair_recv.at[number],
            device_id=(s, partner), device_id_type=MESH)

    def side_copy(place):
        there = lat.at[4 * sp_at(*ORDER[place]) + mine]
        return pltpu.make_async_remote_copy(
            there, there, side_send.at[place], side_recv.at[place],
            device_id=(s, tp_at(1 - 2 * core)), device_id_type=MESH)

    def hand_on(places):
        for place in places:
            side_copy(place).start()
            pair_copy(place, mine, place).start()

    def side_arrived(place):
        there = lat.at[4 * sp_at(pick(place, [pair[0] for pair in ORDER]), pick(place, [pair[1] for pair in ORDER])) + beside]
        pltpu.make_async_remote_copy(
            there, there, side_send.at[place], side_recv.at[place],
            device_id=(s, partner), device_id_type=MESH).wait_recv()
        pltpu.make_async_remote_copy(
            there, there, pair_send.at[16 + place], pair_recv.at[16 + place],
            device_id=(s, partner), device_id_type=MESH).start()

    def out_copy(number, slot, rows, target):
        first, count = rows
        source = w_out.at[pl.ds(first, count)] if number < 9 else w_out_all.at[slot, pl.ds(first, count)]
        return pltpu.make_async_remote_copy(
            source, w_out_all.at[slot, pl.ds(first, count)],
            out_send.at[number], out_recv.at[number],
            device_id=(s, target), device_id_type=MESH)

    whole, upper, lower = (0, 256), (0, 128), (128, 128)
    right, left, across = tp_at(1), tp_at(3), tp_at(2)
    chunks = tuple((64 * chunk, 64) for chunk in range(4))
    out_sends = (
        *((chunk, t, chunks[chunk], right) for chunk in range(4)),
        *((4 + chunk, t, chunks[chunk], left) for chunk in range(4)),
        (8, t, whole, partner),
        (9, right, upper, left), (10, left, lower, right),
        (11, right, whole, partner), (12, left, whole, partner), (13, across, whole, partner),
    )

    def other(slot):
        return (slot // 2) * 2 + 1 - slot % 2

    out_receives = (
        *((chunk, left, chunks[chunk]) for chunk in range(4)),
        *((4 + chunk, right, chunks[chunk]) for chunk in range(4)),
        (8, partner, whole),
        (9, across, upper), (10, across, lower),
        (11, other(right), whole), (12, other(left), whole), (13, other(across), whole),
    )

    def out_chunk(chunk):
        out_copy(*out_sends[3 - chunk]).start()
        out_copy(*out_sends[4 + chunk]).start()

    def out_wait(number):
        _, slot, (first, count) = out_receives[number]
        pltpu.make_async_remote_copy(
            w_out_all.at[slot, pl.ds(first, count)], w_out_all.at[slot, pl.ds(first, count)],
            out_send.at[number], out_recv.at[number],
            device_id=(s, partner), device_id_type=MESH).wait_recv()

    start_phase(0, 0)
    for copy in query_copies():
        copy.start()
    out_copy(*out_sends[8]).start()
    own_out = pltpu.make_async_copy(w_out, w_out_all.at[t], local_sem.at[1])
    own_out.start()

    w_value_t[...] = jnp.transpose(w_value[...].astype(jnp.float32)).astype(jnp.bfloat16)
    top[...] = jnp.full_like(top, masked_score)
    total[...] = jnp.zeros_like(total)
    acc[...] = jnp.zeros_like(acc)

    lanes = lax.broadcasted_iota(jnp.int32, (HALF, 128), 1)

    def set_queries(group, nope_rows, rope_rows):
        wide = rope_rows.astype(jnp.float32)
        turned = pltpu.roll(wide, 64, 1)
        front = lanes < 64
        for head in range(2):
            one = jnp.transpose(nope_rows[:, head * NOPE:(head + 1) * NOPE].astype(jnp.float32))
            low, high = (wide, turned) if head == 0 else (turned, wide)
            for version, tail in enumerate((jnp.where(front, low, 0.0), jnp.where(front, 0.0, high))):
                queries[group, head, version, 0:NOPE, :] = one.astype(jnp.bfloat16)
                queries[group, head, version, NOPE:2 * NOPE, :] = jnp.transpose(tail).astype(jnp.bfloat16)

    hand_on((0,))
    out_chunk(0)
    set_queries(0, nope[pl.ds(0, HALF), :], turned_queries[pl.ds(0, HALF), :])

    def expand(block):
        for chunk in range(4):
            version, side = chunk // 2, chunk % 2
            quarters = (4 * block + 2 * side, 4 * block + 2 * side + 1)
            rows = jnp.concatenate([lat[one, pl.ds(128 * version, 128), :] for one in quarters], axis=0)
            expanded = jnp.dot(rows, w_key[...], preferred_element_type=jnp.float32).astype(jnp.bfloat16)
            for head in range(2):
                keys[head, pl.ds(256 * chunk, 256), 0:NOPE] = expanded[:, head * NOPE:(head + 1) * NOPE]
                for at in range(4):
                    keys[head, pl.ds(256 * chunk + 64 * at, 64), NOPE:2 * NOPE] = (
                        lat[quarters[at // 2], pl.ds(QUARTER, 64), (at % 2) * 128:(at % 2 + 1) * 128])
            values_t[:, 256 * chunk:256 * (chunk + 1)] = lax.dot_general(
                w_value_t[...], rows, (((1,), (1,)), ((), ())), preferred_element_type=jnp.float32
            ).astype(jnp.bfloat16)

    def fold(group, masked):
        def make(piece_at):
            head, first = piece_at // 2, (piece_at % 2) * 256
            largest = top[group, head, :, first:first + 256]
            for chunk in range(4):
                scores = jnp.dot(
                    keys[head, pl.ds(256 * chunk, 256), :],
                    queries[group, head, chunk // 2, :, first:first + 256],
                    preferred_element_type=jnp.float32)
                if masked:
                    row = lax.broadcasted_iota(jnp.int32, scores.shape, 0)
                    key_at = row + jnp.where(row >= 128, 128, 0) + (512 * (chunk % 2) + 128 * (chunk // 2))
                    query_at = lax.broadcasted_iota(jnp.int32, scores.shape, 1) + (first + HALF * group)
                    scores = jnp.where(key_at <= query_at, scores, masked_score)
                held[piece_at % 2, pl.ds(256 * chunk, 256), :] = scores
                largest = jnp.maximum(largest, jnp.max(scores, axis=0, keepdims=True))
            return largest

        after = make(0)
        for piece_at in range(4):
            following = make(piece_at + 1) if piece_at < 3 else None
            head, first = piece_at // 2, (piece_at % 2) * 256
            columns = slice(first, first + 256)
            before = top[group, head, :, columns]
            offset = after * score_base2
            added = jnp.zeros((1, 256), jnp.float32)
            mixed = jnp.zeros((VDIM, 256), jnp.float32)
            for chunk in range(4):
                weights = jnp.exp2(held[piece_at % 2, pl.ds(256 * chunk, 256), :] * score_base2 - offset)
                added += jnp.sum(weights, axis=0, keepdims=True)
                mixed += jnp.dot(
                    values_t[head * VDIM:(head + 1) * VDIM, 256 * chunk:256 * (chunk + 1)],
                    weights.astype(jnp.bfloat16), preferred_element_type=jnp.float32)
            factor = jnp.exp2((before - after) * score_base2)
            total[group, head, :, columns] = total[group, head, :, columns] * factor + added
            acc[group, head, :, columns] = acc[group, head, :, columns] * factor + mixed
            top[group, head, :, columns] = after
            after = following

    def process(block, place):
        @pl.when(block <= jnp.maximum(s, mirror))
        def _():
            expand(block)

        def one(group, carry):
            last = jnp.where(group == 0, s, mirror)

            @pl.when((place == 0) & (group == 1))
            def _():
                wait_received(0, 0)
                start_phase(0, 1)
                hand_on((1, 2, 3, 4))
                start_phase(1, 0)
                for copy in query_copies():
                    copy.wait_recv()
                set_queries(1, far_nope[...], far_rope[...])

            @pl.when(block < last)
            def _():
                fold(group, False)

            @pl.when(block == last)
            def _():
                fold(group, True)

            return carry

        lax.fori_loop(0, 2, one, 0)

    def advance(place, carry):
        @pl.when(place == 1)
        def _():
            wait_received(0, 1, 0, 4)
            start_phase(0, 2)
            hand_on((5, 6))

        @pl.when(place == 2)
        def _():
            wait_received(0, 1, 4, 12)
            start_phase(0, 3)
            hand_on((7, 8, 9, 10))

        @pl.when(place == 5)
        def _():
            wait_received(0, 2)
            wait_received(0, 3)
            start_phase(0, 4)
            hand_on((11, 12, 13, 14))
            wait_received(1, 0)
            start_phase(1, 1)

        @pl.when(place == 9)
        def _():
            wait_received(0, 4)
            hand_on((15,))
            out_chunk(1)
            out_chunk(2)
            out_chunk(3)

        @pl.when(place == 14)
        def _():
            wait_received(1, 1, 0, 4)
            start_phase(1, 2)

        @pl.when(place <= 1)
        def _():
            side_arrived(place)

        @pl.when((place >= 1) & (place < 15))
        def _():
            side_arrived(place + 1)

        dy = pick(place, [pair[0] for pair in ORDER])
        dz = pick(place, [pair[1] for pair in ORDER])
        block = sp_at(dy, dz)
        for number, quarter in ((place, 2 * (x % 2) + 1 - core), (16 + place, 2 * (1 - x % 2) + 1 - core)):
            theirs = lat.at[4 * block + quarter]
            pltpu.make_async_remote_copy(
                theirs, theirs, pair_send.at[number], pair_recv.at[number],
                device_id=(s, partner), device_id_type=MESH).wait_recv()
        process(block, place)
        return carry

    lax.fori_loop(0, 16, advance, 0)

    for group in range(2):
        for head in range(2):
            mixed = acc[group, head] / total[group, head]
            head_out[group, :, head * VDIM:(head + 1) * VDIM] = jnp.transpose(mixed).astype(jnp.bfloat16)

    def head_copy(group, part):
        target = part if group == 0 else 4 + part
        return pltpu.make_async_remote_copy(
            head_out.at[group, pl.ds(128 * part, 128)], heads_all.at[t],
            head_send.at[4 * group + part], head_recv.at[t],
            device_id=(s if group == 0 else mirror, target), device_id_type=MESH)

    for part in range(4):
        head_copy(1, part).start()

        @pl.when(t != part)
        def _():
            head_copy(0, part).start()

    @pl.when(t < 4)
    def _():
        mine = pltpu.make_async_copy(
            head_out.at[0, pl.ds(128 * (t % 4), 128)], heads_all.at[t], local_sem.at[2])
        mine.start()
        mine.wait()

    for number in (2, 3, 4, 5):
        out_wait(number)
    for number in (9, 10):
        out_copy(*out_sends[number]).start()
    wait_received(1, 1, 4, 12)
    start_phase(1, 3)

    def head_wait(slot, carry):
        @pl.when((t >= 4) | (slot != t))
        def _():
            pltpu.make_async_remote_copy(
                head_out.at[0, pl.ds(0, 128)], heads_all.at[slot], head_send.at[0], head_recv.at[slot],
                device_id=(mirror, t), device_id_type=MESH).wait_recv()

        return carry

    own_out.wait()
    for number in (0, 1, 6, 7):
        out_wait(number)
    for number in (11, 12):
        out_copy(*out_sends[number]).start()
    lax.fori_loop(0, 8, head_wait, 0)
    wait_received(1, 2)
    wait_received(1, 3)
    start_phase(1, 4)
    for number in (8, 11, 12):
        out_wait(number)

    stream[...] = resid[...].astype(jnp.float32)

    def project(turn, carry):
        @pl.when(turn == 6)
        def _():
            for number in (9, 10):
                out_wait(number)
            out_copy(*out_sends[13]).start()

        @pl.when(turn == 7)
        def _():
            out_wait(13)

        slot = pick(turn, (0, 1, 2, 3, 6, 7, 4, 5))
        slot = (2 * x + core + slot - 2 * ((core + slot % 2) // 2)) % 8
        stream[...] += jnp.dot(heads_all[slot], w_out_all[slot], preferred_element_type=jnp.float32)
        return carry

    lax.fori_loop(0, 8, project, 0)
    rows_f32 = stream[...]
    scale = lax.rsqrt(jnp.mean(rows_f32 * rows_f32, axis=-1, keepdims=True) + norm_eps)
    rows_all[t] = (rows_f32 * scale * mix_gain[...]).astype(jnp.bfloat16)

    high, low = (0, 64), (64, 64)
    all_rows = (0, 128)
    row_sends = (
        (0, t, all_rows, right), (1, t, all_rows, left), (2, t, all_rows, partner),
        (3, right, high, left), (4, left, low, right),
        (5, right, all_rows, partner), (6, left, all_rows, partner), (7, across, all_rows, partner),
    )
    row_receives = (
        (0, left, all_rows), (1, right, all_rows), (2, partner, all_rows),
        (3, across, high), (4, across, low),
        (5, other(right), all_rows), (6, other(left), all_rows), (7, other(across), all_rows),
    )

    def row_copy(number):
        _, slot, (first, count), target = row_sends[number]
        here = rows_all.at[slot, pl.ds(first, count)]
        return pltpu.make_async_remote_copy(
            here, here, row_send.at[number], row_recv.at[number],
            device_id=(s, target), device_id_type=MESH)

    def row_wait(number):
        _, slot, (first, count) = row_receives[number]
        here = rows_all.at[slot, pl.ds(first, count)]
        pltpu.make_async_remote_copy(
            here, here, row_send.at[number], row_recv.at[number],
            device_id=(s, partner), device_id_type=MESH).wait_recv()

    for number in range(3):
        row_copy(number).start()

    wait_received(1, 4)

    def part_copy(step):
        return pltpu.make_async_remote_copy(
            halves.at[step, 1 - core], got.at[step], part_send.at[step], part_recv.at[step],
            device_id=(s, partner), device_id_type=MESH)

    def chip_total(step):
        part_copy(step).wait_recv()
        return halves[step, core].astype(jnp.float32) + got[step].astype(jnp.float32)

    def sum_copy(number):
        here, there, target = (
            (summed.at[1], arrived.at[0], right),
            (summed.at[2], arrived.at[1], left),
            (summed.at[3, pl.ds(0, 64)], relay.at[0], right),
            (summed.at[3, pl.ds(64, 64)], relay.at[1], left),
            (relay.at[0], arrived.at[2, pl.ds(0, 64)], right),
            (relay.at[1], arrived.at[2, pl.ds(64, 64)], left),
        )[number]
        return pltpu.make_async_remote_copy(
            here, there, sum_send.at[number], sum_recv.at[number],
            device_id=(s, target), device_id_type=MESH)

    def mix(step, carry):
        @pl.when(step == 0)
        def _():
            row_wait(2)

        @pl.when(step == 1)
        def _():
            row_wait(0)
            row_wait(1)
            for number in (3, 4, 5, 6):
                row_copy(number).start()
            row_wait(5)
            row_wait(6)

        @pl.when(step == 2)
        def _():
            row_wait(3)
            row_wait(4)
            row_copy(7).start()

        @pl.when(step == 3)
        def _():
            row_wait(7)

        chip = (x + pick(step, (0, 1, 3, 2))) % SIDE

        def columns(pair, first, count):
            return jnp.concatenate([weights_all[2 * pair + side, pl.ds(first, count), :] for side in range(2)], axis=1)

        def product(first, count):
            added = jnp.zeros((256, count), jnp.float32)
            for pair in range(8):
                rows = rows_all[pl.ds(2 * chip, 2), :, 256 * pair:256 * (pair + 1)].reshape(256, 256)
                added += lax.dot_general(
                    rows, columns(pair, first, count), (((1,), (1,)), ((), ())), preferred_element_type=jnp.float32)
            return added

        for first, count in ((0, 256), (256, 256), (512, 192)):
            gate_value, upward = product(first, count), product(UNITS + first, count)
            hidden[:, first:first + count] = (gate_value / (1.0 + jnp.exp(-gate_value)) * upward).astype(jnp.bfloat16)
        for pair in range(8):
            down = jnp.dot(hidden[...], columns(pair, 2 * UNITS, UNITS), preferred_element_type=jnp.float32)
            halves[step, :, :, 256 * pair:256 * (pair + 1)] = down.astype(jnp.bfloat16).reshape(2, 128, 256)
        part_copy(step).start()

        @pl.when(step == 1)
        def _():
            stream[...] += 0.5 * chip_total(0)

        @pl.when(step == 2)
        def _():
            summed[1] = chip_total(1).astype(jnp.bfloat16)
            sum_copy(0).start()

        @pl.when(step == 3)
        def _():
            summed[2] = chip_total(2).astype(jnp.bfloat16)
            sum_copy(1).start()

        return carry

    lax.fori_loop(0, 4, mix, 0)
    summed[3] = chip_total(3).astype(jnp.bfloat16)
    sum_copy(2).start()
    sum_copy(3).start()
    sum_copy(2).wait_recv()
    sum_copy(4).start()
    sum_copy(3).wait_recv()
    sum_copy(5).start()
    sum_copy(0).wait_recv()
    sum_copy(1).wait_recv()
    stream[...] += 0.5 * (arrived[0].astype(jnp.float32) + arrived[1].astype(jnp.float32))
    sum_copy(4).wait_recv()
    sum_copy(5).wait_recv()
    result[...] = (stream[...] + 0.5 * arrived[2].astype(jnp.float32)).astype(jnp.bfloat16)

    for number in range(6):
        sum_copy(number).wait_send()
    for step in range(4):
        part_copy(step).wait_send()
    for number in range(8):
        row_copy(number).wait_send()
    for number in range(14):
        out_copy(*out_sends[number]).wait_send()
    for copy in query_copies():
        copy.wait_send()
    for phase in range(len(SENDS)):
        for index in range(len(SENDS[phase])):
            shard_copy(0, phase, index).wait_send()
            shard_copy(1, phase, index).wait_send()
    for place in range(16):
        side_copy(place).wait_send()
        pair_copy(place, mine, place).wait_send()
        pair_copy(place, beside, 16 + place).wait_send()
    for number in range(4):
        head_copy(1, number).wait_send()

        @pl.when(t != number)
        def _():
            head_copy(0, number).wait_send()


def layer_call(*operands):
    vmem = pl.BlockSpec(memory_space=pltpu.VMEM)
    anywhere = pl.BlockSpec(memory_space=pl.ANY)
    dma = pltpu.SemaphoreType.DMA
    bf16, f32 = jnp.bfloat16, jnp.float32
    return pl.pallas_call(
        layer_kernel,
        out_shape=jax.ShapeDtypeStruct((128, 2048), bf16),
        in_specs=[anywhere] * len(operands),
        out_specs=vmem,
        scratch_shapes=[
            pltpu.VMEM((ROWS, 256), bf16),
            pltpu.VMEM((ROWS, 128), bf16),
            pltpu.VMEM((QUARTER, 256), bf16),
            pltpu.VMEM((ROPE, QUARTER), bf16),
            pltpu.VMEM((1, 256), f32),
            pltpu.VMEM((256, 256), bf16),
            pltpu.VMEM((256, 256), bf16),
            pltpu.VMEM((128, 2048), bf16),
            pltpu.VMEM((1, 2048), f32),
            pltpu.VMEM((ROWS, 128), f32),
            pltpu.VMEM((ROWS, 128), f32),
            pltpu.VMEM((16, 128), f32),
            pltpu.VMEM((16, 128), f32),
            pltpu.VMEM((ROWS, 128), bf16),
            pltpu.VMEM((64, SHARD, 256), bf16),
            pltpu.VMEM((HALF, 256), bf16),
            pltpu.VMEM((HALF, 128), bf16),
            pltpu.VMEM((2, 2, 2, 256, HALF), bf16),
            pltpu.VMEM((2, ROWS, 256), bf16),
            pltpu.VMEM((256, ROWS), bf16),
            pltpu.VMEM((2, ROWS, 256), f32),
            pltpu.VMEM((256, 256), bf16),
            pltpu.VMEM((2, 2, 1, HALF), f32),
            pltpu.VMEM((2, 2, 1, HALF), f32),
            pltpu.VMEM((2, 2, VDIM, HALF), f32),
            pltpu.VMEM((2, HALF, 256), bf16),
            pltpu.VMEM((8, 128, 256), bf16),
            pltpu.VMEM((8, 256, 2048), bf16),
            pltpu.VMEM((16, 3 * UNITS, 128), bf16),
            pltpu.VMEM((256, UNITS), bf16),
            pltpu.VMEM((128, 2048), f32),
            pltpu.VMEM((8, 128, 2048), bf16),
            pltpu.VMEM((4, 2, 128, 2048), bf16),
            pltpu.VMEM((4, 128, 2048), bf16),
            pltpu.VMEM((4, 128, 2048), bf16),
            pltpu.VMEM((2, 64, 2048), bf16),
            pltpu.VMEM((3, 128, 2048), bf16),
            dma((32,)), dma((64,)), dma((16,)), dma((16,)), dma((32,)), dma((32,)), dma((2,)), dma((2,)),
            dma((8,)), dma((8,)), dma((14,)), dma((14,)), dma((4,)),
            dma((32,)), dma((64,)), dma((8,)), dma((8,)), dma((4,)), dma((4,)), dma((6,)), dma((6,)), dma((16,)),
        ],
        compiler_params=pltpu.CompilerParams(
            collective_id=0, has_side_effects=True, vmem_limit_bytes=67_000_000),
        cost_estimate=pl.CostEstimate(flops=60_000_000_000, bytes_accessed=30_000_000, transcendentals=18_000_000),
        name="layer",
    )(*operands)


def angle_tables(positions):
    frequency = theta_base ** (-2.0 * np.arange(ROPE // 2) / ROPE)
    angle = np.tile(np.asarray(positions, np.float64)[:, None] * frequency[None, :], (1, 4))
    return np.cos(angle).astype(np.float32), np.sin(angle).astype(np.float32)


def on_device(
    resid, query_nope, query_rope, latent, key_rope, latent_gain, w_key, w_value, w_out, mix_gain,
    w_gate, w_up, w_down,
):
    row_tables = angle_tables(np.arange(ROWS))
    block_tables = angle_tables(ROWS * np.arange(16))
    return layer_call(
        query_nope, query_rope, latent, key_rope.T, latent_gain.reshape(1, -1), w_key, w_value, w_out, resid,
        mix_gain.reshape(1, -1), w_gate.T, w_up.T, w_down.T,
        *(jnp.asarray(table) for table in row_tables + block_tables))


def solution(mesh):
    return jax.shard_map(
        on_device,
        mesh=mesh,
        in_specs=(
            P(("sp", "tp"), None),
            P("sp", "tp"),
            P("sp", "tp"),
            P("sp", None),
            P("sp", None),
            P(),
            P(None, "tp"),
            P(None, "tp"),
            P("tp", None),
            P(),
            P("sp", "tp"),
            P("sp", "tp"),
            P("sp", "tp"),
        ),
        out_specs=P(("sp", "tp"), None),
        check_vma=False,
    )
```

time: 180 us -> 155 us (0.86)
  the two profiles are of different devices: /device:TPU:58 before, /device:TPU:1 now
where the time goes in v3:
time: 155 us; the launch traced here: 154 us
  Pallas kernels  152 us (98%)
  local copies, waits for them, and re-layouts  1.88 us (1%)
    pallas_call x1, Pallas kernels, layer_call(): pl.pallas_call(layer_kernel, out_shape=jax.ShapeDtypeStruct((128, 2048),...  152 us

profile of v3, /device:TPU:1, one launch (start us, length us, event | category | flops | bytes accessed | tf_op | source)
XLA Modules:
  0.0 153.8 jit_solution(2630137274862396720)
XLA Ops:
  0.0 151.9 %layer.1 = bf16[128,2048]{1,0:T(8,128)(2,1)} custom-call(bf16[1024,256]{1,0:T(8,128)(2,1)} %nope_in.1, bf16[1024,128]{1,0:T(8,128)(2,1)} %rope_in.1, bf16[1024,256]{1,0:T(8,128)(2,1)} %latent_in.1, bf16[64,1024]{1,0:T(8,128)(2,1)} %bitcast.9, f32[1,256]{1,0:T(1,128)} %bitcast.11, bf16[256,256]{1,0:T(8,128)(2,1)} %w_key_in.1, bf16[256,256]{1,0:T(8,128)(2,1)} %w_value_in.1, ...), custom_call_target="tpu_custom_call" | custom-call | flops 60000002048 | bytes 30000000 | tf_op jit(solution)/shard_map/layer/pallas_call | solution.py:666
  151.9 1.9 %copy.19 = bf16[128,2048]{1,0:T(8,128)(2,1)} copy(bf16[128,2048]{1,0:T(8,128)(2,1)} %layer.1) | data formatting | bytes 1048576

commit v4 on v3

--- a/solution.py
+++ b/solution.py
@@ -14,9 +14,8 @@
 ROWS = 1024
 HALF = 512
 SIDE = 4
-QUARTER = 256
 UNITS = 704
-SHARD = QUARTER + QUARTER // 4
+SHARD = HALF + HALF // 4
 
 norm_eps = 1e-06
 masked_score = -1e30
@@ -74,8 +73,8 @@
     nope, rope, latent, key_rope, gain, w_key, w_value, resid, mix_gain,
     row_cos, row_sin, block_cos, block_sin, turned_queries,
     lat, far_nope, far_rope, queries, keys, values_t, held, w_value_t, top, total, acc, head_out,
-    heads_all, w_out_all, weights_all, hidden, stream, rows_all, halves, got, summed, relay, arrived,
-    send_sem, recv_sem, side_send, side_recv, pair_send, pair_recv, query_send, query_recv, head_send, head_recv,
+    heads_all, w_out_all, weights_all, hidden, stream, rows_all, halves, got, summed, relay, arrived, waiting,
+    send_sem, recv_sem, pair_send, pair_recv, query_send, query_recv, head_send, head_recv,
     out_send, out_recv, local_sem, mixer_send, mixer_recv, row_send, row_recv, part_send, part_recv,
     sum_send, sum_recv, load_sem,
 ):
@@ -92,8 +91,6 @@
         return ((x + dx + SIDE) % SIDE) * 2 + core
 
     partner = x * 2 + 1 - core
-    mine = 2 * (x % 2) + core
-    beside = 2 * (1 - x % 2) + core
 
     barrier = pltpu.get_barrier_semaphore()
     for step in (1, 2, 3):
@@ -104,11 +101,11 @@
     for step in range(8):
         pl.semaphore_signal(barrier, inc=1, device_id=(mirror, (t + step) % 8), device_id_type=MESH)
 
-    quarter_rows = pl.ds(pl.multiple_of((2 * (x % 2) + core) * QUARTER, QUARTER), QUARTER)
+    half_rows = pl.ds(pl.multiple_of(core * HALF, HALF), HALF)
     loads = [
         pltpu.make_async_copy(source, target, load_sem.at[number])
         for number, (source, target) in enumerate((
-            (latent_in.at[quarter_rows], latent), (key_in.at[:, quarter_rows], key_rope), (gain_in, gain),
+            (latent_in.at[half_rows], latent), (key_in.at[:, half_rows], key_rope), (gain_in, gain),
             (block_cos_in, block_cos), (block_sin_in, block_sin), (row_cos_in, row_cos), (row_sin_in, row_sin),
             (rope_in, rope), (nope_in, nope), (w_value_in, w_value), (w_key_in, w_key),
             (gate_in, weights_all.at[s, pl.ds(0, UNITS)]), (up_in, weights_all.at[s, pl.ds(UNITS, UNITS)]),
@@ -129,18 +126,18 @@
         swapped = jnp.where(lane < ROPE // 2, -pltpu.roll(rows_in, 96, 1), pltpu.roll(rows_in, 32, 1))
         return rows_in * cosine + swapped * sine
 
-    own = 4 * s + 2 * (x % 2) + core
+    own = 2 * s + core
     for load in loads[:7]:
         load.wait()
     wide = latent[...].astype(jnp.float32)
     scale = lax.rsqrt(jnp.mean(wide * wide, axis=-1, keepdims=True) + norm_eps)
-    lat[own, pl.ds(0, QUARTER), :] = (wide * scale * gain[...]).astype(jnp.bfloat16)
+    lat[own, pl.ds(0, HALF), :] = (wide * scale * gain[...]).astype(jnp.bfloat16)
     once = key_rope[...].astype(jnp.float32)
-    twice = rotated(jnp.transpose(jnp.concatenate([once, once], axis=0)), (2 * (x % 2) + core) * QUARTER).astype(jnp.bfloat16)
-    front_lanes = lax.broadcasted_iota(jnp.int32, (64, 128), 1) < ROPE
+    twice = rotated(jnp.transpose(jnp.concatenate([once, once], axis=0)), core * HALF).astype(jnp.bfloat16)
+    front_lanes = lax.broadcasted_iota(jnp.int32, (128, 128), 1) < ROPE
     for side in range(2):
-        lat[own, pl.ds(QUARTER, 64), side * 128:(side + 1) * 128] = jnp.where(
-            front_lanes, twice[64 * side:64 * side + 64], twice[128 + 64 * side:192 + 64 * side])
+        lat[own, pl.ds(HALF, 128), side * 128:(side + 1) * 128] = jnp.where(
+            front_lanes, twice[128 * side:128 * side + 128], twice[256 + 128 * side:384 + 128 * side])
     for load in loads[7:9]:
         load.wait()
     for first in (HALF, 0):
@@ -163,7 +160,7 @@
     def piece(kind, block, rows):
         first, count = rows
         if kind == 0:
-            return lat.at[4 * block + mine, pl.ds(first // 2, count // 2)]
+            return lat.at[2 * block + core, pl.ds(first, count)]
         return weights_all.at[block, pl.ds(first * 33 // 10, count * 33 // 10)]
 
     def shard_copy(kind, phase, index):
@@ -176,8 +173,8 @@
             (send_sem, mixer_send)[kind].at[number], (recv_sem, mixer_recv)[kind].at[4 * place + slot],
             device_id=(sp_at(*step), t), device_id_type=MESH)
 
-    def start_phase(kind, phase):
-        for index in range(len(SENDS[phase])):
+    def start_phase(kind, phase, first_index=0, last_index=12):
+        for index in range(len(SENDS[phase]))[first_index:last_index]:
             shard_copy(kind, phase, index).start()
 
     def wait_received(kind, phase, first_index=0, last_index=12):
@@ -189,31 +186,15 @@
                 (send_sem, mixer_send)[kind].at[0], (recv_sem, mixer_recv)[kind].at[4 * place + slot],
                 device_id=(sp_at(*step), t), device_id_type=MESH).wait_recv()
 
-    def pair_copy(place, quarter, number):
-        there = lat.at[4 * sp_at(*ORDER[place]) + quarter]
+    def pair_copy(place):
+        there = lat.at[2 * sp_at(*ORDER[place]) + core]
         return pltpu.make_async_remote_copy(
-            there, there, pair_send.at[number], pair_recv.at[number],
+            there, there, pair_send.at[place], pair_recv.at[place],
             device_id=(s, partner), device_id_type=MESH)
-
-    def side_copy(place):
-        there = lat.at[4 * sp_at(*ORDER[place]) + mine]
-        return pltpu.make_async_remote_copy(
-            there, there, side_send.at[place], side_recv.at[place],
-            device_id=(s, tp_at(1 - 2 * core)), device_id_type=MESH)
 
     def hand_on(places):
         for place in places:
-            side_copy(place).start()
-            pair_copy(place, mine, place).start()
-
-    def side_arrived(place):
-        there = lat.at[4 * sp_at(pick(place, [pair[0] for pair in ORDER]), pick(place, [pair[1] for pair in ORDER])) + beside]
-        pltpu.make_async_remote_copy(
-            there, there, side_send.at[place], side_recv.at[place],
-            device_id=(s, partner), device_id_type=MESH).wait_recv()
-        pltpu.make_async_remote_copy(
-            there, there, pair_send.at[16 + place], pair_recv.at[16 + place],
-            device_id=(s, partner), device_id_type=MESH).start()
+            pair_copy(place).start()
 
     def out_copy(number, slot, rows, target):
         first, count = rows
@@ -282,21 +263,20 @@
                 queries[group, head, version, NOPE:2 * NOPE, :] = jnp.transpose(tail).astype(jnp.bfloat16)
 
     hand_on((0,))
-    out_chunk(0)
+    for chunk in range(4):
+        out_chunk(chunk)
     set_queries(0, nope[pl.ds(0, HALF), :], turned_queries[pl.ds(0, HALF), :])
 
     def expand(block):
-        for chunk in range(4):
-            version, side = chunk // 2, chunk % 2
-            quarters = (4 * block + 2 * side, 4 * block + 2 * side + 1)
-            rows = jnp.concatenate([lat[one, pl.ds(128 * version, 128), :] for one in quarters], axis=0)
+        for plane in range(2):
+            rows = lat[2 * block + plane, pl.ds(0, HALF), :]
             expanded = jnp.dot(rows, w_key[...], preferred_element_type=jnp.float32).astype(jnp.bfloat16)
+            tails = tuple(lat[2 * block + plane, pl.ds(HALF, 128), side * 128:(side + 1) * 128] for side in range(2))
             for head in range(2):
-                keys[head, pl.ds(256 * chunk, 256), 0:NOPE] = expanded[:, head * NOPE:(head + 1) * NOPE]
-                for at in range(4):
-                    keys[head, pl.ds(256 * chunk + 64 * at, 64), NOPE:2 * NOPE] = (
-                        lat[quarters[at // 2], pl.ds(QUARTER, 64), (at % 2) * 128:(at % 2 + 1) * 128])
-            values_t[:, 256 * chunk:256 * (chunk + 1)] = lax.dot_general(
+                keys[head, pl.ds(plane * HALF, HALF), 0:NOPE] = expanded[:, head * NOPE:(head + 1) * NOPE]
+                for quarter in range(4):
+                    keys[head, pl.ds(plane * HALF + quarter * 128, 128), NOPE:2 * NOPE] = tails[quarter % 2]
+            values_t[:, plane * HALF:(plane + 1) * HALF] = lax.dot_general(
                 w_value_t[...], rows, (((1,), (1,)), ((), ())), preferred_element_type=jnp.float32
             ).astype(jnp.bfloat16)
 
@@ -307,11 +287,10 @@
             for chunk in range(4):
                 scores = jnp.dot(
                     keys[head, pl.ds(256 * chunk, 256), :],
-                    queries[group, head, chunk // 2, :, first:first + 256],
+                    queries[group, head, chunk % 2, :, first:first + 256],
                     preferred_element_type=jnp.float32)
                 if masked:
-                    row = lax.broadcasted_iota(jnp.int32, scores.shape, 0)
-                    key_at = row + jnp.where(row >= 128, 128, 0) + (512 * (chunk % 2) + 128 * (chunk // 2))
+                    key_at = lax.broadcasted_iota(jnp.int32, scores.shape, 0) + 256 * chunk
                     query_at = lax.broadcasted_iota(jnp.int32, scores.shape, 1) + (first + HALF * group)
                     scores = jnp.where(key_at <= query_at, scores, masked_score)
                 held[piece_at % 2, pl.ds(256 * chunk, 256), :] = scores
@@ -352,7 +331,6 @@
                 wait_received(0, 0)
                 start_phase(0, 1)
                 hand_on((1, 2, 3, 4))
-                start_phase(1, 0)
                 for copy in query_copies():
                     copy.wait_recv()
                 set_queries(1, far_nope[...], far_rope[...])
@@ -376,59 +354,54 @@
             start_phase(0, 2)
             hand_on((5, 6))
 
-        @pl.when(place == 2)
+        @pl.when(place == 3)
         def _():
             wait_received(0, 1, 4, 12)
             start_phase(0, 3)
             hand_on((7, 8, 9, 10))
-
-        @pl.when(place == 5)
+            start_phase(1, 0)
+
+        @pl.when(place == 6)
         def _():
             wait_received(0, 2)
             wait_received(0, 3)
             start_phase(0, 4)
             hand_on((11, 12, 13, 14))
+            for number in (2, 3, 4, 5):
+                out_wait(number)
+            for number in (9, 10):
+                out_copy(*out_sends[number]).start()
+
+        @pl.when(place == 10)
+        def _():
             wait_received(1, 0)
-            start_phase(1, 1)
-
-        @pl.when(place == 9)
+            start_phase(1, 1, 0, 4)
+            for number in (0, 1, 6, 7):
+                out_wait(number)
+            for number in (11, 12):
+                out_copy(*out_sends[number]).start()
+
+        @pl.when(place == 13)
         def _():
             wait_received(0, 4)
             hand_on((15,))
-            out_chunk(1)
-            out_chunk(2)
-            out_chunk(3)
-
-        @pl.when(place == 14)
-        def _():
-            wait_received(1, 1, 0, 4)
-            start_phase(1, 2)
-
-        @pl.when(place <= 1)
-        def _():
-            side_arrived(place)
-
-        @pl.when((place >= 1) & (place < 15))
-        def _():
-            side_arrived(place + 1)
+            for number in (9, 10):
+                out_wait(number)
+            out_copy(*out_sends[13]).start()
+            start_phase(1, 1, 4, 6)
+            start_phase(1, 1, 8, 10)
 
         dy = pick(place, [pair[0] for pair in ORDER])
         dz = pick(place, [pair[1] for pair in ORDER])
         block = sp_at(dy, dz)
-        for number, quarter in ((place, 2 * (x % 2) + 1 - core), (16 + place, 2 * (1 - x % 2) + 1 - core)):
-            theirs = lat.at[4 * block + quarter]
-            pltpu.make_async_remote_copy(
-                theirs, theirs, pair_send.at[number], pair_recv.at[number],
-                device_id=(s, partner), device_id_type=MESH).wait_recv()
+        theirs = lat.at[2 * block + 1 - core]
+        pltpu.make_async_remote_copy(
+            theirs, theirs, pair_send.at[place], pair_recv.at[place],
+            device_id=(s, partner), device_id_type=MESH).wait_recv()
         process(block, place)
         return carry
 
     lax.fori_loop(0, 16, advance, 0)
-
-    for group in range(2):
-        for head in range(2):
-            mixed = acc[group, head] / total[group, head]
-            head_out[group, :, head * VDIM:(head + 1) * VDIM] = jnp.transpose(mixed).astype(jnp.bfloat16)
 
     def head_copy(group, part):
         target = part if group == 0 else 4 + part
@@ -437,12 +410,19 @@
             head_send.at[4 * group + part], head_recv.at[t],
             device_id=(s if group == 0 else mirror, target), device_id_type=MESH)
 
-    for part in range(4):
-        head_copy(1, part).start()
-
-        @pl.when(t != part)
-        def _():
-            head_copy(0, part).start()
+    def close(group):
+        for head in range(2):
+            mixed = acc[group, head] / total[group, head]
+            head_out[group, :, head * VDIM:(head + 1) * VDIM] = jnp.transpose(mixed).astype(jnp.bfloat16)
+
+    close(1)
+    for number in range(4):
+        head_copy(1, number).start()
+    close(0)
+    for number in range(4):
+        @pl.when(t != number)
+        def _():
+            head_copy(0, number).start()
 
     @pl.when(t < 4)
     def _():
@@ -451,13 +431,6 @@
         mine.start()
         mine.wait()
 
-    for number in (2, 3, 4, 5):
-        out_wait(number)
-    for number in (9, 10):
-        out_copy(*out_sends[number]).start()
-    wait_received(1, 1, 4, 12)
-    start_phase(1, 3)
-
     def head_wait(slot, carry):
         @pl.when((t >= 4) | (slot != t))
         def _():
@@ -467,31 +440,18 @@
 
         return carry
 
+    start_phase(1, 1, 6, 8)
+    start_phase(1, 1, 10, 12)
+    wait_received(1, 1, 0, 4)
+    start_phase(1, 2)
+    for number in (8, 11, 12, 13):
+        out_wait(number)
     own_out.wait()
-    for number in (0, 1, 6, 7):
-        out_wait(number)
-    for number in (11, 12):
-        out_copy(*out_sends[number]).start()
     lax.fori_loop(0, 8, head_wait, 0)
-    wait_received(1, 2)
-    wait_received(1, 3)
-    start_phase(1, 4)
-    for number in (8, 11, 12):
-        out_wait(number)
 
     stream[...] = resid[...].astype(jnp.float32)
 
     def project(turn, carry):
-        @pl.when(turn == 6)
-        def _():
-            for number in (9, 10):
-                out_wait(number)
-            out_copy(*out_sends[13]).start()
-
-        @pl.when(turn == 7)
-        def _():
-            out_wait(13)
-
         slot = pick(turn, (0, 1, 2, 3, 6, 7, 4, 5))
         slot = (2 * x + core + slot - 2 * ((core + slot % 2) // 2)) % 8
         stream[...] += jnp.dot(heads_all[slot], w_out_all[slot], preferred_element_type=jnp.float32)
@@ -505,14 +465,16 @@
     high, low = (0, 64), (64, 64)
     all_rows = (0, 128)
     row_sends = (
-        (0, t, all_rows, right), (1, t, all_rows, left), (2, t, all_rows, partner),
+        (0, t, low, right), (1, t, high, left), (2, t, all_rows, partner),
         (3, right, high, left), (4, left, low, right),
         (5, right, all_rows, partner), (6, left, all_rows, partner), (7, across, all_rows, partner),
+        (8, t, high, right), (9, t, low, left),
     )
     row_receives = (
-        (0, left, all_rows), (1, right, all_rows), (2, partner, all_rows),
+        (0, left, low), (1, right, high), (2, partner, all_rows),
         (3, across, high), (4, across, low),
         (5, other(right), all_rows), (6, other(left), all_rows), (7, other(across), all_rows),
+        (8, left, high), (9, right, low),
     )
 
     def row_copy(number):
@@ -531,7 +493,24 @@
 
     for number in range(3):
         row_copy(number).start()
-
+    row_wait(0)
+    row_wait(1)
+    for number in (3, 4, 8, 9):
+        row_copy(number).start()
+    wait_received(1, 1, 4, 12)
+    start_phase(1, 3)
+    row_wait(2)
+    row_wait(3)
+    row_wait(4)
+    row_copy(7).start()
+    wait_received(1, 2)
+    wait_received(1, 3)
+    start_phase(1, 4)
+    row_wait(8)
+    row_wait(9)
+    row_copy(5).start()
+    row_copy(6).start()
+    row_wait(7)
     wait_received(1, 4)
 
     def part_copy(step):
@@ -545,42 +524,41 @@
 
     def sum_copy(number):
         here, there, target = (
-            (summed.at[1], arrived.at[0], right),
-            (summed.at[2], arrived.at[1], left),
-            (summed.at[3, pl.ds(0, 64)], relay.at[0], right),
-            (summed.at[3, pl.ds(64, 64)], relay.at[1], left),
-            (relay.at[0], arrived.at[2, pl.ds(0, 64)], right),
-            (relay.at[1], arrived.at[2, pl.ds(64, 64)], left),
+            (summed.at[0, pl.ds(0, 64)], relay.at[0], right),
+            (summed.at[0, pl.ds(64, 64)], relay.at[1], left),
+            (summed.at[1, pl.ds(64, 64)], arrived.at[0, pl.ds(64, 64)], right),
+            (summed.at[2, pl.ds(0, 64)], arrived.at[1, pl.ds(0, 64)], left),
+            (summed.at[1, pl.ds(0, 64)], arrived.at[0, pl.ds(0, 64)], right),
+            (summed.at[2, pl.ds(64, 64)], arrived.at[1, pl.ds(64, 64)], left),
         )[number]
         return pltpu.make_async_remote_copy(
             here, there, sum_send.at[number], sum_recv.at[number],
             device_id=(s, target), device_id_type=MESH)
 
+    def finish(step):
+        if step == 3:
+            stream[...] += 0.5 * chip_total(3)
+        elif step == 0:
+            summed[0] = chip_total(0).astype(jnp.bfloat16)
+            sum_copy(0).start()
+            sum_copy(1).start()
+        else:
+            total_rows = chip_total(step)
+            sent, kept = (slice(64, 128), slice(0, 64)) if step == 1 else (slice(0, 64), slice(64, 128))
+            summed[step, sent, :] = total_rows[sent].astype(jnp.bfloat16)
+            sum_copy(step + 1).start()
+            waiting[step - 1] = total_rows[kept]
+
     def mix(step, carry):
-        @pl.when(step == 0)
-        def _():
-            row_wait(2)
-
         @pl.when(step == 1)
         def _():
-            row_wait(0)
-            row_wait(1)
-            for number in (3, 4, 5, 6):
-                row_copy(number).start()
             row_wait(5)
+
+        @pl.when(step == 2)
+        def _():
             row_wait(6)
 
-        @pl.when(step == 2)
-        def _():
-            row_wait(3)
-            row_wait(4)
-            row_copy(7).start()
-
-        @pl.when(step == 3)
-        def _():
-            row_wait(7)
-
-        chip = (x + pick(step, (0, 1, 3, 2))) % SIDE
+        chip = (x + pick(step, (2, 1, 3, 0))) % SIDE
 
         def columns(pair, first, count):
             return jnp.concatenate([weights_all[2 * pair + side, pl.ds(first, count), :] for side in range(2)], axis=1)
@@ -596,47 +574,38 @@
         for first, count in ((0, 256), (256, 256), (512, 192)):
             gate_value, upward = product(first, count), product(UNITS + first, count)
             hidden[:, first:first + count] = (gate_value / (1.0 + jnp.exp(-gate_value)) * upward).astype(jnp.bfloat16)
+
+        for one in range(3):
+            @pl.when(step == one + 1)
+            def _():
+                finish(one)
+
         for pair in range(8):
             down = jnp.dot(hidden[...], columns(pair, 2 * UNITS, UNITS), preferred_element_type=jnp.float32)
             halves[step, :, :, 256 * pair:256 * (pair + 1)] = down.astype(jnp.bfloat16).reshape(2, 128, 256)
         part_copy(step).start()
 
-        @pl.when(step == 1)
-        def _():
-            stream[...] += 0.5 * chip_total(0)
-
-        @pl.when(step == 2)
-        def _():
-            summed[1] = chip_total(1).astype(jnp.bfloat16)
-            sum_copy(0).start()
-
-        @pl.when(step == 3)
-        def _():
-            summed[2] = chip_total(2).astype(jnp.bfloat16)
-            sum_copy(1).start()
-
         return carry
 
     lax.fori_loop(0, 4, mix, 0)
-    summed[3] = chip_total(3).astype(jnp.bfloat16)
-    sum_copy(2).start()
-    sum_copy(3).start()
+    for side in range(2):
+        sum_copy(side).wait_recv()
+        rows = pl.ds(64 * side, 64)
+        summed[1 + side, rows, :] = (waiting[side] + relay[side].astype(jnp.float32)).astype(jnp.bfloat16)
+        sum_copy(4 + side).start()
+    finish(3)
     sum_copy(2).wait_recv()
-    sum_copy(4).start()
     sum_copy(3).wait_recv()
-    sum_copy(5).start()
-    sum_copy(0).wait_recv()
-    sum_copy(1).wait_recv()
-    stream[...] += 0.5 * (arrived[0].astype(jnp.float32) + arrived[1].astype(jnp.float32))
     sum_copy(4).wait_recv()
     sum_copy(5).wait_recv()
-    result[...] = (stream[...] + 0.5 * arrived[2].astype(jnp.float32)).astype(jnp.bfloat16)
+    result[...] = (
+        stream[...] + 0.5 * (arrived[0].astype(jnp.float32) + arrived[1].astype(jnp.float32))).astype(jnp.bfloat16)
 
     for number in range(6):
         sum_copy(number).wait_send()
     for step in range(4):
         part_copy(step).wait_send()
-    for number in range(8):
+    for number in range(10):
         row_copy(number).wait_send()
     for number in range(14):
         out_copy(*out_sends[number]).wait_send()
@@ -647,9 +616,7 @@
             shard_copy(0, phase, index).wait_send()
             shard_copy(1, phase, index).wait_send()
     for place in range(16):
-        side_copy(place).wait_send()
-        pair_copy(place, mine, place).wait_send()
-        pair_copy(place, beside, 16 + place).wait_send()
+        pair_copy(place).wait_send()
     for number in range(4):
         head_copy(1, number).wait_send()
 
@@ -671,8 +638,8 @@
         scratch_shapes=[
             pltpu.VMEM((ROWS, 256), bf16),
             pltpu.VMEM((ROWS, 128), bf16),
-            pltpu.VMEM((QUARTER, 256), bf16),
-            pltpu.VMEM((ROPE, QUARTER), bf16),
+            pltpu.VMEM((HALF, 256), bf16),
+            pltpu.VMEM((ROPE, HALF), bf16),
             pltpu.VMEM((1, 256), f32),
             pltpu.VMEM((256, 256), bf16),
             pltpu.VMEM((256, 256), bf16),
@@ -683,7 +650,7 @@
             pltpu.VMEM((16, 128), f32),
             pltpu.VMEM((16, 128), f32),
             pltpu.VMEM((ROWS, 128), bf16),
-            pltpu.VMEM((64, SHARD, 256), bf16),
+            pltpu.VMEM((32, SHARD, 256), bf16),
             pltpu.VMEM((HALF, 256), bf16),
             pltpu.VMEM((HALF, 128), bf16),
             pltpu.VMEM((2, 2, 2, 256, HALF), bf16),
@@ -703,12 +670,13 @@
             pltpu.VMEM((8, 128, 2048), bf16),
             pltpu.VMEM((4, 2, 128, 2048), bf16),
             pltpu.VMEM((4, 128, 2048), bf16),
-            pltpu.VMEM((4, 128, 2048), bf16),
+            pltpu.VMEM((3, 128, 2048), bf16),
             pltpu.VMEM((2, 64, 2048), bf16),
-            pltpu.VMEM((3, 128, 2048), bf16),
-            dma((32,)), dma((64,)), dma((16,)), dma((16,)), dma((32,)), dma((32,)), dma((2,)), dma((2,)),
+            pltpu.VMEM((2, 128, 2048), bf16),
+            pltpu.VMEM((2, 64, 2048), f32),
+            dma((32,)), dma((64,)), dma((16,)), dma((16,)), dma((2,)), dma((2,)),
             dma((8,)), dma((8,)), dma((14,)), dma((14,)), dma((4,)),
-            dma((32,)), dma((64,)), dma((8,)), dma((8,)), dma((4,)), dma((4,)), dma((6,)), dma((6,)), dma((16,)),
+            dma((32,)), dma((64,)), dma((10,)), dma((10,)), dma((4,)), dma((4,)), dma((6,)), dma((6,)), dma((16,)),
         ],
         compiler_params=pltpu.CompilerParams(
             collective_id=0, has_side_effects=True, vmem_limit_bytes=67_000_000),

time: 155 us -> 139 us (0.90)
  Pallas kernels: 152 us -> 137 us
    pallas_call x1, Pallas kernels: 152 us -> 137 us  [layer_call(): pl.pallas_call(layer_kernel, out_shape=jax.ShapeDtypeStruct((128, 2048),...]
where the time goes in v4:
time: 139 us
  Pallas kernels  137 us (99%)
  local copies, waits for them, and re-layouts  1.88 us (1%)
    pallas_call x1, Pallas kernels, layer_call(): pl.pallas_call(layer_kernel, out_shape=jax.ShapeDtypeStruct((128, 2048),...  137 us

profile of v4, /device:TPU:1, one launch (start us, length us, event | category | flops | bytes accessed | tf_op | source)
XLA Modules:
  0.0 139.1 jit_solution(14752686039710735094)
XLA Ops:
  0.0 137.2 %layer.1 = bf16[128,2048]{1,0:T(8,128)(2,1)} custom-call(bf16[1024,256]{1,0:T(8,128)(2,1)} %nope_in.1, bf16[1024,128]{1,0:T(8,128)(2,1)} %rope_in.1, bf16[1024,256]{1,0:T(8,128)(2,1)} %latent_in.1, bf16[64,1024]{1,0:T(8,128)(2,1)} %bitcast.9, f32[1,256]{1,0:T(1,128)} %bitcast.11, bf16[256,256]{1,0:T(8,128)(2,1)} %w_key_in.1, bf16[256,256]{1,0:T(8,128)(2,1)} %w_value_in.1, ...), custom_call_target="tpu_custom_call" | custom-call | flops 60000002048 | bytes 30000000 | tf_op jit(solution)/shard_map/layer/pallas_call | solution.py:633
  137.2 1.9 %copy.19 = bf16[128,2048]{1,0:T(8,128)(2,1)} copy(bf16[128,2048]{1,0:T(8,128)(2,1)} %layer.1) | data formatting | bytes 1048576

commit v5 on v4

--- a/solution.py
+++ b/solution.py
@@ -107,7 +107,9 @@
         for number, (source, target) in enumerate((
             (latent_in.at[half_rows], latent), (key_in.at[:, half_rows], key_rope), (gain_in, gain),
             (block_cos_in, block_cos), (block_sin_in, block_sin), (row_cos_in, row_cos), (row_sin_in, row_sin),
-            (rope_in, rope), (nope_in, nope), (w_value_in, w_value), (w_key_in, w_key),
+            *((rope_in.at[pl.ds(128 * one, 128)], rope.at[pl.ds(HALF * (one % 2) + 128 * (one // 2), 128)]) for one in range(8)),
+            *((nope_in.at[pl.ds(128 * one, 128)], nope.at[pl.ds(HALF * (one % 2) + 128 * (one // 2), 128)]) for one in range(8)),
+            (w_value_in, w_value), (w_key_in, w_key),
             (gate_in, weights_all.at[s, pl.ds(0, UNITS)]), (up_in, weights_all.at[s, pl.ds(UNITS, UNITS)]),
             (down_in, weights_all.at[s, pl.ds(2 * UNITS, UNITS)]), (resid_in, resid), (mix_gain_in, mix_gain),
         ))
@@ -138,12 +140,13 @@
     for side in range(2):
         lat[own, pl.ds(HALF, 128), side * 128:(side + 1) * 128] = jnp.where(
             front_lanes, twice[128 * side:128 * side + 128], twice[256 + 128 * side:384 + 128 * side])
-    for load in loads[7:9]:
+    for load in loads[7:23]:
         load.wait()
-    for first in (HALF, 0):
-        turned_queries[pl.ds(first, HALF), :] = rotated(
-            rope[pl.ds(first, HALF), :].astype(jnp.float32), first).astype(jnp.bfloat16)
-    for load in loads[9:]:
+    for one in (1, 3, 5, 7, 0, 2, 4, 6):
+        held_rows = pl.ds(HALF * (one % 2) + 128 * (one // 2), 128)
+        turned_queries[held_rows, :] = rotated(
+            rope[held_rows, :].astype(jnp.float32), 128 * one).astype(jnp.bfloat16)
+    for load in loads[23:]:
         load.wait()
     pl.semaphore_wait(barrier, 21)
 
@@ -291,7 +294,8 @@
                     preferred_element_type=jnp.float32)
                 if masked:
                     key_at = lax.broadcasted_iota(jnp.int32, scores.shape, 0) + 256 * chunk
-                    query_at = lax.broadcasted_iota(jnp.int32, scores.shape, 1) + (first + HALF * group)
+                    column = lax.broadcasted_iota(jnp.int32, scores.shape, 1)
+                    query_at = column + jnp.where(column >= 128, 128, 0) + (2 * first + 128 * group)
                     scores = jnp.where(key_at <= query_at, scores, masked_score)
                 held[piece_at % 2, pl.ds(256 * chunk, 256), :] = scores
                 largest = jnp.maximum(largest, jnp.max(scores, axis=0, keepdims=True))
@@ -374,12 +378,17 @@
 
         @pl.when(place == 10)
         def _():
-            wait_received(1, 0)
-            start_phase(1, 1, 0, 4)
             for number in (0, 1, 6, 7):
                 out_wait(number)
             for number in (11, 12):
                 out_copy(*out_sends[number]).start()
+
+        @pl.when(place == 12)
+        def _():
+            wait_received(1, 0)
+            start_phase(1, 1, 0, 4)
+            start_phase(1, 1, 4, 6)
+            start_phase(1, 1, 8, 10)
 
         @pl.when(place == 13)
         def _():
@@ -388,8 +397,6 @@
             for number in (9, 10):
                 out_wait(number)
             out_copy(*out_sends[13]).start()
-            start_phase(1, 1, 4, 6)
-            start_phase(1, 1, 8, 10)
 
         dy = pick(place, [pair[0] for pair in ORDER])
         dz = pick(place, [pair[1] for pair in ORDER])
@@ -404,7 +411,7 @@
     lax.fori_loop(0, 16, advance, 0)
 
     def head_copy(group, part):
-        target = part if group == 0 else 4 + part
+        target = 2 * part + group
         return pltpu.make_async_remote_copy(
             head_out.at[group, pl.ds(128 * part, 128)], heads_all.at[t],
             head_send.at[4 * group + part], head_recv.at[t],
@@ -420,25 +427,23 @@
         head_copy(1, number).start()
     close(0)
     for number in range(4):
-        @pl.when(t != number)
+        @pl.when(t != 2 * number)
         def _():
             head_copy(0, number).start()
 
-    @pl.when(t < 4)
+    @pl.when(core == 0)
     def _():
         mine = pltpu.make_async_copy(
-            head_out.at[0, pl.ds(128 * (t % 4), 128)], heads_all.at[t], local_sem.at[2])
+            head_out.at[0, pl.ds(128 * x, 128)], heads_all.at[t], local_sem.at[2])
         mine.start()
         mine.wait()
 
-    def head_wait(slot, carry):
-        @pl.when((t >= 4) | (slot != t))
+    def head_wait(slot):
+        @pl.when((core == 1) | (slot != t))
         def _():
             pltpu.make_async_remote_copy(
                 head_out.at[0, pl.ds(0, 128)], heads_all.at[slot], head_send.at[0], head_recv.at[slot],
                 device_id=(mirror, t), device_id_type=MESH).wait_recv()
-
-        return carry
 
     start_phase(1, 1, 6, 8)
     start_phase(1, 1, 10, 12)
@@ -447,13 +452,13 @@
     for number in (8, 11, 12, 13):
         out_wait(number)
     own_out.wait()
-    lax.fori_loop(0, 8, head_wait, 0)
 
     stream[...] = resid[...].astype(jnp.float32)
 
     def project(turn, carry):
         slot = pick(turn, (0, 1, 2, 3, 6, 7, 4, 5))
         slot = (2 * x + core + slot - 2 * ((core + slot % 2) // 2)) % 8
+        head_wait(slot)
         stream[...] += jnp.dot(heads_all[slot], w_out_all[slot], preferred_element_type=jnp.float32)
         return carry
 
@@ -493,25 +498,21 @@
 
     for number in range(3):
         row_copy(number).start()
+    wait_received(1, 1, 4, 12)
+    start_phase(1, 3)
     row_wait(0)
     row_wait(1)
     for number in (3, 4, 8, 9):
         row_copy(number).start()
-    wait_received(1, 1, 4, 12)
-    start_phase(1, 3)
+    wait_received(1, 2)
+    wait_received(1, 3)
+    start_phase(1, 4)
     row_wait(2)
     row_wait(3)
     row_wait(4)
     row_copy(7).start()
-    wait_received(1, 2)
-    wait_received(1, 3)
-    start_phase(1, 4)
-    row_wait(8)
-    row_wait(9)
-    row_copy(5).start()
-    row_copy(6).start()
+    wait_received(1, 4)
     row_wait(7)
-    wait_received(1, 4)
 
     def part_copy(step):
         return pltpu.make_async_remote_copy(
@@ -552,6 +553,10 @@
     def mix(step, carry):
         @pl.when(step == 1)
         def _():
+            row_wait(8)
+            row_wait(9)
+            row_copy(5).start()
+            row_copy(6).start()
             row_wait(5)
 
         @pl.when(step == 2)
@@ -620,7 +625,7 @@
     for number in range(4):
         head_copy(1, number).wait_send()
 
-        @pl.when(t != number)
+        @pl.when(t != 2 * number)
         def _():
             head_copy(0, number).wait_send()
 
@@ -676,7 +681,7 @@
             pltpu.VMEM((2, 64, 2048), f32),
             dma((32,)), dma((64,)), dma((16,)), dma((16,)), dma((2,)), dma((2,)),
             dma((8,)), dma((8,)), dma((14,)), dma((14,)), dma((4,)),
-            dma((32,)), dma((64,)), dma((10,)), dma((10,)), dma((4,)), dma((4,)), dma((6,)), dma((6,)), dma((16,)),
+            dma((32,)), dma((64,)), dma((10,)), dma((10,)), dma((4,)), dma((4,)), dma((6,)), dma((6,)), dma((30,)),
         ],
         compiler_params=pltpu.CompilerParams(
             collective_id=0, has_side_effects=True, vmem_limit_bytes=67_000_000),

time: 139 us -> 135 us (0.971)
  Pallas kernels: 137 us -> 133 us
    pallas_call x1, Pallas kernels: 137 us -> 133 us  [layer_call(): pl.pallas_call(layer_kernel, out_shape=jax.ShapeDtypeStruct((128, 2048),...]
where the time goes in v5:
time: 135 us; the launch traced here: 134 us
  Pallas kernels  133 us (99%)
  local copies, waits for them, and re-layouts  1.88 us (1%)
    pallas_call x1, Pallas kernels, layer_call(): pl.pallas_call(layer_kernel, out_shape=jax.ShapeDtypeStruct((128, 2048),...  133 us

profile of v5, /device:TPU:1, one launch (start us, length us, event | category | flops | bytes accessed | tf_op | source)
XLA Modules:
  0.0 134.5 jit_solution(18294477068503953156)
XLA Ops:
  0.0 132.6 %layer.1 = bf16[128,2048]{1,0:T(8,128)(2,1)} custom-call(bf16[1024,256]{1,0:T(8,128)(2,1)} %nope_in.1, bf16[1024,128]{1,0:T(8,128)(2,1)} %rope_in.1, bf16[1024,256]{1,0:T(8,128)(2,1)} %latent_in.1, bf16[64,1024]{1,0:T(8,128)(2,1)} %bitcast.9, f32[1,256]{1,0:T(1,128)} %bitcast.11, bf16[256,256]{1,0:T(8,128)(2,1)} %w_key_in.1, bf16[256,256]{1,0:T(8,128)(2,1)} %w_value_in.1, ...), custom_call_target="tpu_custom_call" | custom-call | flops 60000002048 | bytes 30000000 | tf_op jit(solution)/shard_map/layer/pallas_call | solution.py:638
  132.6 1.9 %copy.19 = bf16[128,2048]{1,0:T(8,128)(2,1)} copy(bf16[128,2048]{1,0:T(8,128)(2,1)} %layer.1) | data formatting | bytes 1048576

commit v6 on v5

--- a/solution.py
+++ b/solution.py
@@ -74,7 +74,7 @@
     row_cos, row_sin, block_cos, block_sin, turned_queries,
     lat, far_nope, far_rope, queries, keys, values_t, held, w_value_t, top, total, acc, head_out,
     heads_all, w_out_all, weights_all, hidden, stream, rows_all, halves, got, summed, relay, arrived, waiting,
-    send_sem, recv_sem, pair_send, pair_recv, query_send, query_recv, head_send, head_recv,
+    send_sem, recv_sem, side_send, side_recv, pair_send, pair_recv, query_send, query_recv, head_send, head_recv,
     out_send, out_recv, local_sem, mixer_send, mixer_recv, row_send, row_recv, part_send, part_recv,
     sum_send, sum_recv, load_sem,
 ):
@@ -160,9 +160,14 @@
                 device_id=(mirror, t), device_id_type=MESH),
         )
 
-    def piece(kind, block, rows):
+    even_odd = x % 2
+
+    def piece(kind, block, rows, split=False):
         first, count = rows
         if kind == 0:
+            if split:
+                first = first // 320 * 320 + 160 * even_odd + (first % 320) // 2
+                return lat.at[2 * block + core, pl.ds(pl.multiple_of(first, 16), count // 2)]
             return lat.at[2 * block + core, pl.ds(first, count)]
         return weights_all.at[block, pl.ds(first * 33 // 10, count * 33 // 10)]
 
@@ -170,7 +175,7 @@
         source, rows, step, slot = SENDS[phase][index]
         number = sum(len(one) for one in SENDS[:phase]) + index
         place = at_receiver(source, step)
-        there = piece(kind, sp_at(*source), rows)
+        there = piece(kind, sp_at(*source), rows, phase > 1 or phase == 1 and index > 3)
         return pltpu.make_async_remote_copy(
             there, there,
             (send_sem, mixer_send)[kind].at[number], (recv_sem, mixer_recv)[kind].at[4 * place + slot],
@@ -181,9 +186,9 @@
             shard_copy(kind, phase, index).start()
 
     def wait_received(kind, phase, first_index=0, last_index=12):
-        for source, rows, step, slot in SENDS[phase][first_index:last_index]:
+        for index, (source, rows, step, slot) in list(enumerate(SENDS[phase]))[first_index:last_index]:
             place = at_receiver(source, step)
-            there = piece(kind, sp_at(*ORDER[place]), rows)
+            there = piece(kind, sp_at(*ORDER[place]), rows, phase > 1 or phase == 1 and index > 3)
             pltpu.make_async_remote_copy(
                 there, there,
                 (send_sem, mixer_send)[kind].at[0], (recv_sem, mixer_recv)[kind].at[4 * place + slot],
@@ -197,7 +202,31 @@
 
     def hand_on(places):
         for place in places:
-            pair_copy(place).start()
+            if place < 7:
+                pair_copy(place).start()
+            else:
+                side_copy(place, 0).start()
+                side_copy(place, 1).start()
+
+    def side_copy(place, part):
+        there = piece(0, sp_at(*ORDER[place]), (ALPHA, BETA)[part], True)
+        number = 2 * (place - 7) + part
+        return pltpu.make_async_remote_copy(
+            there, there, side_send.at[number], side_recv.at[number],
+            device_id=(s, tp_at(1 - 2 * core)), device_id_type=MESH)
+
+    def side_arrived(place):
+        block = 2 * sp_at(pick(place, [pair[0] for pair in ORDER]), pick(place, [pair[1] for pair in ORDER])) + core
+        for part in range(2):
+            first = pl.multiple_of(320 * part + 160 * (1 - even_odd), 16)
+            there = lat.at[block, pl.ds(first, 160)]
+            number = 2 * (place - 7) + part
+            pltpu.make_async_remote_copy(
+                there, there, side_send.at[number], side_recv.at[number],
+                device_id=(s, partner), device_id_type=MESH).wait_recv()
+        pltpu.make_async_remote_copy(
+            lat.at[block], lat.at[block], pair_send.at[place], pair_recv.at[place],
+            device_id=(s, partner), device_id_type=MESH).start()
 
     def out_copy(number, slot, rows, target):
         first, count = rows
@@ -365,7 +394,7 @@
             hand_on((7, 8, 9, 10))
             start_phase(1, 0)
 
-        @pl.when(place == 6)
+        @pl.when(place == 5)
         def _():
             wait_received(0, 2)
             wait_received(0, 3)
@@ -376,14 +405,14 @@
             for number in (9, 10):
                 out_copy(*out_sends[number]).start()
 
-        @pl.when(place == 10)
+        @pl.when(place == 8)
         def _():
             for number in (0, 1, 6, 7):
                 out_wait(number)
             for number in (11, 12):
                 out_copy(*out_sends[number]).start()
 
-        @pl.when(place == 12)
+        @pl.when(place == 10)
         def _():
             wait_received(1, 0)
             start_phase(1, 1, 0, 4)
@@ -392,11 +421,17 @@
 
         @pl.when(place == 13)
         def _():
+            start_phase(1, 1, 6, 8)
+            start_phase(1, 1, 10, 12)
+
+        @pl.when(place == 11)
+        def _():
             wait_received(0, 4)
             hand_on((15,))
-            for number in (9, 10):
-                out_wait(number)
-            out_copy(*out_sends[13]).start()
+
+        @pl.when((place >= 6) & (place < 15))
+        def _():
+            side_arrived(place + 1)
 
         dy = pick(place, [pair[0] for pair in ORDER])
         dz = pick(place, [pair[1] for pair in ORDER])
@@ -445,17 +480,22 @@
                 head_out.at[0, pl.ds(0, 128)], heads_all.at[slot], head_send.at[0], head_recv.at[slot],
                 device_id=(mirror, t), device_id_type=MESH).wait_recv()
 
-    start_phase(1, 1, 6, 8)
-    start_phase(1, 1, 10, 12)
     wait_received(1, 1, 0, 4)
     start_phase(1, 2)
-    for number in (8, 11, 12, 13):
+    for number in (9, 10):
+        out_wait(number)
+    out_copy(*out_sends[13]).start()
+    for number in (8, 11, 12):
         out_wait(number)
     own_out.wait()
 
     stream[...] = resid[...].astype(jnp.float32)
 
     def project(turn, carry):
+        @pl.when(turn == 7)
+        def _():
+            out_wait(13)
+
         slot = pick(turn, (0, 1, 2, 3, 6, 7, 4, 5))
         slot = (2 * x + core + slot - 2 * ((core + slot % 2) // 2)) % 8
         head_wait(slot)
@@ -500,13 +540,25 @@
         row_copy(number).start()
     wait_received(1, 1, 4, 12)
     start_phase(1, 3)
+
+    def last_weights():
+        wait_received(1, 2)
+        wait_received(1, 3)
+        start_phase(1, 4)
+
+    @pl.when(core == 1)
+    def _():
+        last_weights()
+
     row_wait(0)
     row_wait(1)
     for number in (3, 4, 8, 9):
         row_copy(number).start()
-    wait_received(1, 2)
-    wait_received(1, 3)
-    start_phase(1, 4)
+
+    @pl.when(core == 0)
+    def _():
+        last_weights()
+
     row_wait(2)
     row_wait(3)
     row_wait(4)
@@ -622,6 +674,9 @@
             shard_copy(1, phase, index).wait_send()
     for place in range(16):
         pair_copy(place).wait_send()
+        if place > 6:
+            side_copy(place, 0).wait_send()
+            side_copy(place, 1).wait_send()
     for number in range(4):
         head_copy(1, number).wait_send()
 
@@ -679,7 +734,7 @@
             pltpu.VMEM((2, 64, 2048), bf16),
             pltpu.VMEM((2, 128, 2048), bf16),
             pltpu.VMEM((2, 64, 2048), f32),
-            dma((32,)), dma((64,)), dma((16,)), dma((16,)), dma((2,)), dma((2,)),
+            dma((32,)), dma((64,)), dma((18,)), dma((18,)), dma((16,)), dma((16,)), dma((2,)), dma((2,)),
             dma((8,)), dma((8,)), dma((14,)), dma((14,)), dma((4,)),
             dma((32,)), dma((64,)), dma((10,)), dma((10,)), dma((4,)), dma((4,)), dma((6,)), dma((6,)), dma((30,)),
         ],

time: 135 us -> 134 us (level)
  no operation moved by 1% of the time
where the time goes in v6:
time: 134 us
  Pallas kernels  132 us (99%)
  local copies, waits for them, and re-layouts  1.88 us (1%)
    pallas_call x1, Pallas kernels, layer_call(): pl.pallas_call(layer_kernel, out_shape=jax.ShapeDtypeStruct((128, 2048),...  132 us

profile of v6, /device:TPU:1, one launch (start us, length us, event | category | flops | bytes accessed | tf_op | source)
XLA Modules:
  0.0 134.2 jit_solution(16135153184906114894)
XLA Ops:
  0.0 132.3 %layer.1 = bf16[128,2048]{1,0:T(8,128)(2,1)} custom-call(bf16[1024,256]{1,0:T(8,128)(2,1)} %nope_in.1, bf16[1024,128]{1,0:T(8,128)(2,1)} %rope_in.1, bf16[1024,256]{1,0:T(8,128)(2,1)} %latent_in.1, bf16[64,1024]{1,0:T(8,128)(2,1)} %bitcast.9, f32[1,256]{1,0:T(1,128)} %bitcast.11, bf16[256,256]{1,0:T(8,128)(2,1)} %w_key_in.1, bf16[256,256]{1,0:T(8,128)(2,1)} %w_value_in.1, ...), custom_call_target="tpu_custom_call" | custom-call | flops 60000002048 | bytes 30000000 | tf_op jit(solution)/shard_map/layer/pallas_call | solution.py:693
  132.3 1.9 %copy.19 = bf16[128,2048]{1,0:T(8,128)(2,1)} copy(bf16[128,2048]{1,0:T(8,128)(2,1)} %layer.1) | data formatting | bytes 1048576
